TPU v7x, 32 devices: a whole 2x2x4 slice. The times are simulated.
32 devices in a mesh: sp: 8 (over z, x), tp: 4 (over y, core).
Axes of the slice: x: 2, y: 2, z: 4, core: 2. Of those that a mesh axis runs over, the one named last changes fastest.
Arguments:
- moe_input: bfloat16 [2048, 2048], P('sp'), may hold values from -6 to 6
- out_cotangent: bfloat16 [2048, 2048], P('sp'), may hold values from -6 to 6
- routes: int32 [2048, 2], P('sp'), may hold values from 0 to 7, all different within a row; in each aligned block of 256 rows (0 to 255, 256 to 511, ...) at most 96 rows name the same one
- group_weight: float32 [2048], P('sp'), may hold values from 0.5 to 1
- inner_weight: float32 [2048, 2], P('sp'), may hold values from 0.3 to 1
- gate_weight: bfloat16 [8, 2048, 1024], P('sp', None, 'tp'), may hold values from -0.125 to 0.125
- up_weight: bfloat16 [8, 2048, 1024], P('sp', None, 'tp'), may hold values from -0.125 to 0.125
- down_weight: bfloat16 [8, 1024, 2048], P('sp', 'tp'), may hold values from -0.1875 to 0.1875
- value_in: bfloat16 [2048, 1024], P('sp', 'tp'), may hold values from -6 to 6
- gate_in: bfloat16 [2048, 1024], P('sp', 'tp'), may hold values from -6 to 6
- conv_taps: bfloat16 [31, 1024], P(None, 'tp'), may hold values from -1 to 1
- norm_hat: bfloat16 [2048, 1024], P('sp', 'tp'), may hold values from -6 to 6
- norm_rstd: float32 [2048], P('sp'), may hold values from 0.3 to 3
- norm_gain: float32 [1024], P('tp'), may hold values from 0.1 to 1.9
- out_proj: bfloat16 [2048, 1024], P(None, 'tp'), may hold values from -0.1875 to 0.1875
Outputs:
- gate_grad: bfloat16 [8, 2048, 1024], P('sp', None, 'tp')
- up_grad: bfloat16 [8, 2048, 1024], P('sp', None, 'tp')
- down_grad: bfloat16 [8, 1024, 2048], P('sp', 'tp')
- proj_grad: float32 [2048, 1024], P('sp', 'tp')
- value_grad: bfloat16 [2048, 1024], P('sp', 'tp')
- gate_in_grad: bfloat16 [2048, 1024], P('sp', 'tp')
Inputs may be any that keep to these rules, and one draw needn't show every extreme that they name: In the rows of one device (aligned blocks of 256 tokens) no expert is named by more than 96 routes, and in every draw some expert is named by exactly 96 in some block; a token's two experts differ.
All inputs are finite; a program needn't handle non-finite values.
Results may differ from a plain program's by a relative error of at most 0.009.
Values may be sent and summed in bfloat16 or wider, within the bound.
No kernel may reach another device: no remote copies, remote signals or barrier semaphores. Data moves between devices by JAX's collectives and lax.ppermute only.
A program may use at most 128 MiB of HBM per device.

v0:
```python
import functools

import jax
import jax.numpy as jnp
from jax import lax
from jax.experimental import pallas as pl
from jax.experimental.pallas import tpu as pltpu
from jax.sharding import PartitionSpec as P


F32 = jnp.float32
BF16 = jnp.bfloat16
VMEM = pl.BlockSpec(memory_space=pltpu.VMEM)
SMEM = pl.BlockSpec(memory_space=pltpu.SMEM)
HBM = pl.BlockSpec(memory_space=pltpu.HBM)


WIDE = 3
GROUPS = {"a": ((0, 1, 2), ()), "b": ((4,), (3, 5)), "c": ((), (6, 7))}
PLACES = sum((g[0] for g in GROUPS.values()), ()) + sum((g[1] for g in GROUPS.values()), ())
SENT = ((5, 7), (1, 3), (4, 6), (0, 2))


def swapped(block, axis, mask):
    count = lax.axis_size(axis)
    return lax.ppermute(block, axis, [(i, i ^ mask) for i in range(count)])


def shifted(block, axis, distance):
    devices = range(lax.axis_size(axis))
    route = [(i - distance, i) for i in devices if i - distance in devices]
    return lax.ppermute(block, axis, route)


def silu_slope(logits, squashed):
    return squashed * (1.0 + logits * (1.0 - squashed))


def dot(a, b, contract):
    return lax.dot_general(a, b, ((contract[:1], contract[1:]), ((), ())), preferred_element_type=F32)


def params(mib):
    return pltpu.CompilerParams(vmem_limit_bytes=mib * 1024 * 1024)


def array(*shape, kind=BF16):
    return jax.ShapeDtypeStruct(shape, kind)


def in_hbm(*arrays):
    return [pltpu.with_memory_space_constraint(a, pltpu.HBM) for a in arrays]


def dispatch_kernel(
    experts, capacity, wide, flip, pos, routes_in, group_in, inner_in, x_all, g_all, select_ref, g_own, *refs
):
    slot_refs, (x_own, x_far, g_far, routes, group, inner, sems) = refs[:-7], refs[-7:]
    tables = [
        pltpu.make_async_copy(source, target, sems.at[4 + i])
        for i, (source, target) in enumerate(
            ((routes_in, routes), (group_in, group), (inner_in, inner))
        )
    ]
    for copy in tables:
        copy.start()
    width = x_own.shape[1]

    def fetch(source, target, quarter, i):
        at = pl.ds(pl.multiple_of(quarter * width, width), width)
        return pltpu.make_async_copy(source.at[:, at], target, sems.at[i])

    far = jnp.bitwise_xor(pos[0], 2)
    copies = [fetch(x_all, x_own, pos[0], 0), fetch(g_all, g_own, pos[0], 1)]
    if wide:
        copies += [fetch(x_all, x_far, far, 2), fetch(g_all, g_far, far, 3)]
    for copy in copies:
        copy.start()
    for copy in tables:
        copy.wait()
    tokens = routes.shape[1]
    slots = experts * capacity
    expert = lax.broadcasted_iota(jnp.int32, (experts, tokens), 0)
    earlier = lax.broadcasted_iota(jnp.int32, (tokens, tokens), 0)
    later = lax.broadcasted_iota(jnp.int32, (tokens, tokens), 1)
    before = (earlier < later).astype(F32).astype(BF16)
    slot_number = lax.broadcasted_iota(jnp.int32, (slots, tokens), 0)
    base = jnp.zeros((experts, 1), F32)
    select = jnp.zeros((slots, tokens), F32)
    weight = jnp.zeros((slots, tokens), F32)
    for k in range(2):
        route = routes[k : k + 1, :]
        hot = (expert == route).astype(F32)
        counts = dot(hot.astype(BF16), before, (1, 0)) + base
        base = base + jnp.sum(hot, axis=1, keepdims=True)
        rank = jnp.sum(hot * counts, axis=0, keepdims=True).astype(jnp.int32)
        owner = route
        if flip:
            mask = jnp.bitwise_xor(route, pos[1])
            owner = mask
            for place, own in enumerate(PLACES):
                if place != own:
                    owner = jnp.where(mask == own, place, owner)
        hit = slot_number == owner * capacity + rank
        select = jnp.where(hit, 1.0, select)
        weight = jnp.where(hit, group[...] * inner[k : k + 1, :], weight)
    select = select.astype(BF16)
    select_ref[...] = select
    weight = jnp.sum(weight, axis=1, keepdims=True)
    rows = slots // len(slot_refs)
    for copy in copies:
        copy.wait()
    picked_x = dot(select, x_own[...], (1, 0)).astype(BF16)
    picked_g = (weight * dot(select, g_own[...], (1, 0))).astype(BF16)
    for i, out in enumerate(slot_refs):
        out[:, :width] = picked_x[i * rows : (i + 1) * rows]
        out[:, width : 2 * width] = picked_g[i * rows : (i + 1) * rows]
    if wide:
        select, weight = select[: wide * rows], weight[: wide * rows]
        picked_x = dot(select, x_far[...], (1, 0)).astype(BF16)
        picked_g = (weight * dot(select, g_far[...], (1, 0))).astype(BF16)
        for i, out in enumerate(slot_refs[:wide]):
            out[:, 2 * width : 3 * width] = picked_x[i * rows : (i + 1) * rows]
            out[:, 3 * width :] = picked_g[i * rows : (i + 1) * rows]


def dispatch(pos, routes, group_weight, inner_weight, x, g, experts, capacity, parts, wide):
    tokens, model = x.shape
    width = model // lax.axis_size("tp")
    slots = experts * capacity
    rows = slots // parts
    return pl.pallas_call(
        functools.partial(dispatch_kernel, experts, capacity, wide, parts > 1),
        in_specs=[SMEM] + [HBM] * 5,
        out_specs=[VMEM] * (2 + parts),
        out_shape=[array(slots, tokens), array(tokens, width)]
        + [array(rows, (4 if i < wide else 2) * width) for i in range(parts)],
        scratch_shapes=[pltpu.VMEM((tokens, width), BF16)] * 3
        + [
            pltpu.VMEM((2, tokens), jnp.int32),
            pltpu.VMEM((1, tokens), F32),
            pltpu.VMEM((2, tokens), F32),
            pltpu.SemaphoreType.DMA((7,)),
        ],
        compiler_params=params(20),
        name="dispatch",
    )(pos, *in_hbm(routes.T, group_weight[None, :], inner_weight.T, x, g))


def quarters(pos, width):
    p = pos[0]
    order = [p, jnp.bitwise_xor(p, 2), jnp.bitwise_xor(p, 1), jnp.bitwise_xor(p, 3)]
    return [pl.multiple_of(q * width, width) for q in order]


def expert_kernel(layout, fetch, pos, *refs):
    if fetch:
        refs, (fetched, sem) = refs[:-2], refs[-2:]
    ins, (wg, wu, wd, both, send, keep, gd, ud, ha) = refs[:-9], refs[-9:]
    if fetch:
        copy = pltpu.make_async_copy(wd, fetched, sem)
        copy.start()
    width = keep.shape[1] // 2
    model = both.shape[1] // 2
    order = quarters(pos, width)
    for ref, (row, which) in zip(ins, layout):
        rows = slice(row, row + ref.shape[0])
        for i in range(ref.shape[1] // (2 * width)):
            at = order[which + i]
            lower = 2 * i * width
            both[rows, pl.ds(at, width)] = ref[:, lower : lower + width]
            at = pl.multiple_of(model + at, width)
            both[rows, pl.ds(at, width)] = ref[:, lower + width : lower + 2 * width]
    gate = dot(both[:, :model], wg[...], (1, 0))
    up = dot(both[:, :model], wu[...], (1, 0))
    if fetch:
        copy.wait()
        wd = fetched
    act = dot(both[:, model:], wd[...], (1, 1))
    sigma = jax.nn.sigmoid(gate)
    ha[...] = (gate * sigma * up).astype(BF16)
    gate_delta = (act * up * silu_slope(gate, sigma)).astype(BF16)
    up_delta = (act * gate * sigma).astype(BF16)
    gd[...] = gate_delta
    ud[...] = up_delta

    def partial_of(at):
        value = dot(gate_delta, wg[pl.ds(at, width), :], (1, 1))
        value = value + dot(up_delta, wu[pl.ds(at, width), :], (1, 1))
        return value.astype(BF16)

    send[:, :width] = partial_of(order[2])
    send[:, width:] = partial_of(order[3])
    keep[:, :width] = partial_of(order[0])
    keep[:, width:] = partial_of(order[1])


def expert_math(pos, blocks, layout, rows, wg, wu, wd, fetch):
    model, hidden = wg.shape
    width = model // lax.axis_size("tp")
    return pl.pallas_call(
        functools.partial(expert_kernel, layout, fetch),
        in_specs=[SMEM] + [VMEM] * (len(blocks) + 2) + [HBM if fetch else VMEM],
        out_specs=[VMEM] * 6,
        out_shape=[array(rows, 2 * model)]
        + [array(rows, 2 * width)] * 2
        + [array(rows, hidden)] * 3,
        scratch_shapes=[pltpu.VMEM(wd.shape, BF16), pltpu.SemaphoreType.DMA] if fetch else [],
        compiler_params=params(20),
        name="expert",
    )(pos, *blocks, wg, wu, *(in_hbm(wd) if fetch else [wd]))


def weight_kernel(groups, *refs):
    ins, (gate_grad, up_grad, down_grad) = refs[: 4 * groups], refs[4 * groups :]
    model = gate_grad.shape[0]
    hidden = gate_grad.shape[1]
    width = model // 4
    for at in range(0, model, width):
        gate = jnp.zeros((width, hidden), F32)
        up = jnp.zeros((width, hidden), F32)
        down = jnp.zeros((hidden, width), F32)
        for i in range(groups):
            both, gd, ud, ha = ins[4 * i : 4 * i + 4]
            part = both[:, at : at + width]
            gate = gate + dot(part, gd[...], (0, 0))
            up = up + dot(part, ud[...], (0, 0))
            down = down + dot(ha[...], both[:, model + at : model + at + width], (0, 0))
        gate_grad[at : at + width, :] = gate.astype(BF16)
        up_grad[at : at + width, :] = up.astype(BF16)
        down_grad[:, at : at + width] = down.astype(BF16)


def weight_math(flat, model, hidden):
    return pl.pallas_call(
        functools.partial(weight_kernel, len(flat) // 4),
        in_specs=[VMEM] * len(flat),
        out_specs=[VMEM] * 3,
        out_shape=[array(model, hidden), array(model, hidden), array(hidden, model)],
        compiler_params=params(20),
        name="weights",
    )(*flat)


def join_kernel(keep, mate, *outs):
    row = 0
    for out in outs:
        rows = slice(row, row + out.shape[0])
        out[...] = (keep[rows, :].astype(F32) + mate[rows, :].astype(F32)).astype(BF16)
        row += out.shape[0]


def join(keep, mate, rows, parts):
    return pl.pallas_call(
        join_kernel,
        in_specs=[VMEM] * 2,
        out_specs=[VMEM] * parts,
        out_shape=[array(rows, keep.shape[1])] * parts,
        compiler_params=params(12),
        name="join",
    )(keep, mate)


def fold_kernel(start, keep, mate, half, far):
    width = half.shape[1]
    half[...] = keep[start:, :width].astype(F32) + mate[start:, :width].astype(F32)
    far[...] = (keep[start:, width:].astype(F32) + mate[start:, width:].astype(F32)).astype(BF16)


def fold(keep, mate, start):
    rows, double = keep.shape
    shape = (rows - start, double // 2)
    return pl.pallas_call(
        functools.partial(fold_kernel, start),
        in_specs=[VMEM] * 2,
        out_specs=[VMEM] * 2,
        out_shape=[array(*shape, kind=F32), array(*shape)],
        compiler_params=params(12),
        name="fold",
    )(keep, mate)


def stacked(blocks, rows):
    at = 0
    for block in blocks:
        rows[at : at + block.shape[0], :] = block[...]
        at += block.shape[0]


def early_kernel(select, *refs):
    blocks, (keep, far, rows) = refs[:-3], refs[-3:]
    stacked(blocks, rows)
    width = keep.shape[1]
    total = dot(select[: rows.shape[0], :], rows[...], (0, 0))
    keep[...] = total[:, :width]
    far[...] = total[:, width:].astype(BF16)


def early(select, blocks):
    tokens = select.shape[1]
    rows = sum(b.shape[0] for b in blocks)
    width = blocks[0].shape[1] // 2
    return pl.pallas_call(
        early_kernel,
        in_specs=[VMEM] * (1 + len(blocks)),
        out_specs=[VMEM] * 2,
        out_shape=[array(tokens, width, kind=F32), array(tokens, width)],
        scratch_shapes=[pltpu.VMEM((rows, 2 * width), BF16)],
        compiler_params=params(12),
        name="early",
    )(select, *blocks)


def combine_kernel(count, select, g_own, *refs):
    blocks, others, (out, rows) = refs[:count], refs[count:-2], refs[-2:]
    stacked(blocks, rows)
    total = dot(select[select.shape[0] - rows.shape[0] :, :], rows[...], (0, 0))
    for other in others:
        total = total + other[...].astype(F32)
    out[...] = (g_own[...].astype(F32) + total).astype(BF16)


def combine(select, g, blocks, others):
    tokens = select.shape[1]
    width = blocks[0].shape[1]
    rows = sum(b.shape[0] for b in blocks)
    return pl.pallas_call(
        functools.partial(combine_kernel, len(blocks)),
        in_specs=[VMEM] * (2 + len(blocks) + len(others)),
        out_specs=VMEM,
        out_shape=array(tokens, width),
        scratch_shapes=[pltpu.VMEM((rows, width), BF16)],
        compiler_params=params(12),
        name="combine",
    )(select, g, *blocks, *others)


def project_kernel(pos, own, far, mate, mate_far, hat, gain, mixer, *refs):
    outs, total = refs[:-1], refs[-1]
    width = own.shape[1]
    normed = hat[...].astype(F32) * gain[...]
    act = (normed * jax.nn.sigmoid(normed)).astype(BF16)
    for buf, at in zip((own, far, mate, mate_far), quarters(pos, width)):
        part = buf[...]
        mixer[:, pl.ds(at, width)] = part
        total[pl.ds(at, width), :] = dot(part, act, (0, 0))
    if len(outs) == 1:
        outs[0][...] = total[...].astype(BF16)
        return
    for out, masks in zip(outs, SENT):
        rows = out.shape[0] // len(masks)
        for i, mask in enumerate(masks):
            at = pl.multiple_of(jnp.bitwise_xor(pos[1], mask) * rows, rows)
            out[i * rows : (i + 1) * rows, :] = total[pl.ds(at, rows), :].astype(out.dtype)


def project(pos, bufs, norm_hat, norm_gain, parts):
    tokens, width = bufs[0].shape
    model = width * lax.axis_size("tp")
    channels = norm_hat.shape[1]
    outs = [array(model, channels)]
    if parts > 1:
        rows = model // parts
        outs = [array(len(m) * rows, channels, kind=k) for m, k in zip(SENT, (BF16, BF16, F32, F32))]
    return pl.pallas_call(
        project_kernel,
        in_specs=[SMEM] + [VMEM] * 6,
        out_specs=[VMEM] * (1 + len(outs)),
        out_shape=[array(tokens, model)] + outs,
        scratch_shapes=[pltpu.VMEM((model, channels), F32)],
        compiler_params=params(12),
        name="project",
    )(pos, *bufs, norm_hat, norm_gain[None, :])


def added(a, b):
    return a.astype(F32) + b.astype(F32)


def exchanged(block, width):
    count = lax.axis_size("sp")
    shape = block.shape
    block = block.reshape(count, shape[0] // count, width)
    return lax.all_to_all(block, "sp", split_axis=0, concat_axis=0, tiled=True).reshape(shape)


def returned_rows(pos, args, weights):
    moe_input, _, _, _, _ = args
    tok_rows, model_width = moe_input.shape
    sp_count = lax.axis_size("sp")
    capacity = 3 * tok_rows // sp_count
    width = model_width // lax.axis_size("tp")
    ring = sp_count == 8
    parts, wide = (sp_count, WIDE) if ring else (1, 0)
    select, g_own, *slots = dispatch(pos, *args[2:], *args[:2], sp_count, capacity, parts, wide)
    arrived, far, mate, mate_far = {}, {}, {}, {}
    if ring:
        for d, block in zip(PLACES, slots):
            arrived[d] = swapped(block, "sp", d) if d else block
    else:
        arrived[0] = exchanged(slots[0], 2 * width)
    for d, block in arrived.items():
        mate[d] = swapped(block, "tp", 1)
        if d not in PLACES[:wide]:
            far[d] = swapped(block, "tp", 2)
            mate_far[d] = swapped(far[d], "tp", 1)
    flat, plane = [], []

    def experts(group, name):
        rows = arrived[group[0]].shape[0]
        ins, layout = [], []
        for i, d in enumerate(group):
            ins += [arrived[d], mate[d]]
            layout += [(i * rows, 0), (i * rows, 2)]
            if d in far:
                ins += [far[d], mate_far[d]]
                layout += [(i * rows, 1), (i * rows, 3)]
        both, send, keep, *rest = expert_math(
            pos, ins, layout, rows * len(group), *weights, name == "a"
        )
        flat.extend([both] + rest)
        return keep, swapped(send, "tp", 1)

    finals = []
    for name, (direct, routed) in GROUPS.items() if ring else [("c", ((), (0,)))]:
        keep, mates = experts(direct + routed, name)
        rows = keep.shape[0] // len(direct + routed)
        if direct:
            sums = join(keep, mates, rows, len(direct))
            for d, block in zip(direct, sums):
                plane.append(swapped(block, "sp", d) if d else block)
        if routed:
            half, to_far = fold(keep, mates, rows * len(direct))
            to_far = swapped(to_far, "tp", 2)
            sums = join(half, to_far, rows, len(routed))
            for d, block in zip(routed, sums):
                finals.append(swapped(block, "sp", d) if ring else exchanged(block, width))
    others = []
    if plane:
        own, away = early(select, plane)
        others = [own, swapped(away, "tp", 2)]
    grads = weight_math(flat, model_width, weights[0].shape[1])
    return combine(select, g_own, finals, others), grads


def on_device(
    moe_input,
    out_cotangent,
    routes,
    group_weight,
    inner_weight,
    gate_weight,
    up_weight,
    down_weight,
    value_in,
    gate_in,
    conv_taps,
    norm_hat,
    norm_rstd,
    norm_gain,
    out_proj,
):
    tok_rows, model_width = moe_input.shape
    sp_count = lax.axis_size("sp")
    tp_count = lax.axis_size("tp")
    if gate_weight.shape[0] != 1 or tp_count != 4:
        raise ValueError("unsupported mesh")
    pos = jnp.stack([lax.axis_index("tp"), lax.axis_index("sp")]).astype(jnp.int32)
    mixer_part, grads = returned_rows(
        pos,
        (moe_input, out_cotangent, routes, group_weight, inner_weight),
        (gate_weight[0], up_weight[0], down_weight[0]),
    )
    parts = sp_count if sp_count == 8 else 1
    mixer_far = swapped(mixer_part, "tp", 2)
    mixer_mate = swapped(mixer_part, "tp", 1)
    mixer_mate_far = swapped(mixer_far, "tp", 1)
    bufs = (mixer_part, mixer_far, mixer_mate, mixer_mate_far)
    mixer_grad, *blocks = project(pos, bufs, norm_hat, norm_gain, parts)
    if parts > 1:
        away, close, kept_away, kept = blocks
        away = swapped(away, "sp", 1)
        close = swapped(close, "sp", 1)
        far = join(kept_away, away, model_width // parts, 2)
        rows = model_width // parts
        near = added(kept[rows:], close[rows:]).astype(BF16)
        proj_grad = added(kept[:rows], close[:rows])
        for d, block in ((2, near), (4, far[0]), (6, far[1])):
            proj_grad = proj_grad + swapped(block, "sp", d).astype(F32)
    else:
        block = blocks[0].reshape(sp_count, model_width // sp_count, -1)
        block = lax.all_to_all(block, "sp", split_axis=0, concat_axis=0, tiled=True)
        proj_grad = jnp.sum(block.astype(F32), axis=0)
    normed = norm_hat.astype(F32) * norm_gain[None, :]
    norm_sigma = jax.nn.sigmoid(normed)
    silu_grad = jnp.dot(mixer_grad, out_proj, preferred_element_type=F32)
    hat_grad = silu_grad * silu_slope(normed, norm_sigma) * norm_gain[None, :]
    norm_values = norm_hat.astype(F32)
    sums = jnp.stack([jnp.sum(hat_grad, axis=1), jnp.sum(hat_grad * norm_values, axis=1)])
    sums = sums + swapped(sums, "tp", 1)
    grad_sum, grad_dot = sums + swapped(sums, "tp", 2)
    channels = norm_values.shape[1] * tp_count
    conv_grad = norm_rstd[:, None] * (
        hat_grad - grad_sum[:, None] / channels - norm_values * (grad_dot[:, None] / channels)
    )
    tap_count = conv_taps.shape[0]
    incoming = shifted(conv_grad[: tap_count - 1], "sp", -1)
    tap_values = conv_taps.astype(F32)
    short = tap_count - 1
    extended = jnp.concatenate([conv_grad, jnp.zeros_like(incoming)], axis=0)
    glu_grad = jnp.zeros_like(conv_grad)
    for offset in range(tap_count):
        lower = short - offset
        glu_grad = glu_grad + tap_values[offset][None, :] * extended[lower : lower + tok_rows]
    glu_grad = lax.optimization_barrier(glu_grad)
    extended = jnp.concatenate([jnp.zeros_like(incoming), incoming], axis=0)
    edge = jnp.zeros_like(incoming)
    for offset in range(tap_count):
        lower = short - offset
        edge = edge + tap_values[offset][None, :] * extended[lower : lower + short]
    glu_grad = glu_grad + jnp.pad(edge, ((tok_rows - short, 0), (0, 0)))
    input_sigma = jax.nn.sigmoid(gate_in.astype(F32))
    value_grad = (glu_grad * input_sigma).astype(BF16)
    gate_in_grad = (
        glu_grad * value_in.astype(F32) * input_sigma * (1.0 - input_sigma)
    ).astype(BF16)
    return (*(grad[None] for grad in grads), proj_grad, value_grad, gate_in_grad)


def solution(mesh):
    return jax.shard_map(
        on_device,
        mesh=mesh,
        in_specs=(
            P("sp", None),
            P("sp", None),
            P("sp", None),
            P("sp"),
            P("sp", None),
            P("sp", None, "tp"),
            P("sp", None, "tp"),
            P("sp", "tp", None),
            P("sp", "tp"),
            P("sp", "tp"),
            P(None, "tp"),
            P("sp", "tp"),
            P("sp"),
            P("tp"),
            P(None, "tp"),
        ),
        out_specs=(
            P("sp", None, "tp"),
            P("sp", None, "tp"),
            P("sp", "tp", None),
            P("sp", "tp"),
            P("sp", "tp"),
            P("sp", "tp"),
        ),
        check_vma=False,
    )
```

profile of v0, /device:TPU:0, one launch (start us, length us, event | category | flops | bytes accessed | tf_op | source)
XLA Modules:
  0.0 147.0 jit_solution(11929285908048336859)
XLA Ops:
  0.7 2.7 %dispatch.1 = (bf16[768,256]{1,0:T(8,128)(2,1)S(1)}, bf16[256,512]{1,0:T(8,128)(2,1)S(1)}, bf16[96,2048]{1,0:T(8,128)(2,1)S(1)}, bf16[96,2048]{1,0:T(8,128)(2,1)...) custom-call(s32[2]{0:T(128)S(1)} %pad_add_fusion.1.pos, ...), custom_call_target="tpu_custom_call" | custom-call | tf_op jit(solution)/shard_map/dispatch/pallas_call | solution.py:132
  3.4 4.0 %collective-permute-start.9 = (bf16[96,1024]{1,0:T(8,128)(2,1)S(1)}, bf16[96,1024]{1,0:T(8,128)(2,1)S(1)}, u32[]{:S(2)}, u32[]{:S(2)}) collective-permute-start(bf16[96,1024]{1,0:T(8,128)(2,1)S(1)} %get-tuple-element.65), channel_id=1, source_target_pairs={{0,12},{4,8},{8,4},{12,0},{16,28},{20,24},{24,20},{28,16},{1,13},{... | collective-permute-start | bytes 589832 | tf_op jit(solution)/shard_map/ppermute | solution.py:26
  7.5 2.6 %collective-permute-start.13 = (bf16[96,1024]{1,0:T(8,128)(2,1)S(1)}, bf16[96,1024]{1,0:T(8,128)(2,1)S(1)}, u32[]{:S(2)}, u32[]{:S(2)}) collective-permute-start(bf16[96,1024]{1,0:T(8,128)(2,1)S(1)} %get-tuple-element.66), channel_id=1, source_target_pairs={{0,20},{4,16},{8,28},{12,24},{16,4},{20,0},{24,12},{28,8},{1,21},{... | collective-permute-start | bytes 589832 | tf_op jit(solution)/shard_map/ppermute | solution.py:26
  10.4 2.5 %collective-permute-start.17 = (bf16[96,1024]{1,0:T(8,128)(2,1)S(1)}, bf16[96,1024]{1,0:T(8,128)(2,1)S(1)}, u32[]{:S(2)}, u32[]{:S(2)}) collective-permute-start(bf16[96,1024]{1,0:T(8,128)(2,1)S(1)} %get-tuple-element.71), channel_id=1, source_target_pairs={{0,24},{4,28},{8,16},{12,20},{16,8},{20,12},{24,0},{28,4},{1,25},{... | collective-permute-start | bytes 589832 | tf_op jit(solution)/shard_map/ppermute | solution.py:26
  12.8 2.3 %collective-permute-start.21 = (bf16[96,1024]{1,0:T(8,128)(2,1)S(1)}, bf16[96,1024]{1,0:T(8,128)(2,1)S(1)}, u32[]{:S(2)}, u32[]{:S(2)}) collective-permute-start(bf16[96,1024]{1,0:T(8,128)(2,1)S(1)} %get-tuple-element.72), channel_id=1, source_target_pairs={{0,28},{4,24},{8,20},{12,16},{16,12},{20,8},{24,4},{28,0},{1,29},{... | collective-permute-start | bytes 589832 | tf_op jit(solution)/shard_map/ppermute | solution.py:26
  15.2 1.8 %collective-permute-start.11 = (bf16[96,1024]{1,0:T(8,128)(2,1)S(1)}, bf16[96,1024]{1,0:T(8,128)(2,1)S(1)}, u32[]{:S(2)}, u32[]{:S(2)}) collective-permute-start(bf16[96,1024]{1,0:T(8,128)(2,1)S(1)} %collective-permute-done.9.refs_4_), channel_id=1, source_target_pairs={{0,2},{1,3},{2,0},{3,1},{4,6},{5,7},{6,4},{7,5},{8,10},{9,11},{10,... | collective-permute-start | bytes 589832 | tf_op jit(solution)/shard_map/ppermute | solution.py:26
  17.0 16.9 %collective-permute-done.13.refs_8_ = bf16[96,1024]{1,0:T(8,128)(2,1)S(1)} collective-permute-done((bf16[96,1024]{1,0:T(8,128)(2,1)S(1)}, bf16[96,1024]{1,0:T(8,128)(2,1)S(1)}, u32[]{:S(2)}, u32[]{:S(2)}) %collective-permute-start.13) | collective-permute-done | bytes 196640 | tf_op jit(solution)/shard_map/ppermute | solution.py:26
  33.9 1.5 %collective-permute-start.15 = (bf16[96,1024]{1,0:T(8,128)(2,1)S(1)}, bf16[96,1024]{1,0:T(8,128)(2,1)S(1)}, u32[]{:S(2)}, u32[]{:S(2)}) collective-permute-start(bf16[96,1024]{1,0:T(8,128)(2,1)S(1)} %collective-permute-done.13.refs_8_), channel_id=1, source_target_pairs={{0,2},{1,3},{2,0},{3,1},{4,6},{5,7},{6,4},{7,5},{8,10},{9,11},{10,... | collective-permute-start | bytes 589832 | tf_op jit(solution)/shard_map/ppermute | solution.py:26
  35.4 1.8 %collective-permute-done.5.refs_0_ = bf16[96,1024]{1,0:T(8,128)(2,1)S(1)} collective-permute-done((bf16[96,1024]{1,0:T(8,128)(2,1)S(1)}, bf16[96,1024]{1,0:T(8,128)(2,1)S(1)}, u32[]{:S(2)}, u32[]{:S(2)}) %collective-permute-start.5) | collective-permute-done | bytes 196640 | tf_op jit(solution)/shard_map/ppermute | solution.py:26
  38.7 3.3 %collective-permute-start.3 = (bf16[96,2048]{1,0:T(8,128)(2,1)S(1)}, bf16[96,2048]{1,0:T(8,128)(2,1)S(1)}, u32[]{:S(2)}, u32[]{:S(2)}) collective-permute-start(bf16[96,2048]{1,0:T(8,128)(2,1)S(1)} %get-tuple-element.59), channel_id=1, source_target_pairs={{0,8},{4,12},{8,0},{12,4},{16,24},{20,28},{24,16},{28,20},{1,9},{5... | collective-permute-start | bytes 1179656 | tf_op jit(solution)/shard_map/ppermute | solution.py:26
  41.9 1.5 %collective-permute-start.7 = (bf16[96,1024]{1,0:T(8,128)(2,1)S(1)}, bf16[96,1024]{1,0:T(8,128)(2,1)S(1)}, u32[]{:S(2)}, u32[]{:S(2)}) collective-permute-start(bf16[96,1024]{1,0:T(8,128)(2,1)S(1)} %collective-permute-done.5.refs_0_), channel_id=1, source_target_pairs={{0,2},{1,3},{2,0},{3,1},{4,6},{5,7},{6,4},{7,5},{8,10},{9,11},{10,... | collective-permute-start | bytes 589832 | tf_op jit(solution)/shard_map/ppermute | solution.py:26
  44.0 3.6 %collective-permute-done.7.refs_2_ = bf16[96,1024]{1,0:T(8,128)(2,1)S(1)} collective-permute-done((bf16[96,1024]{1,0:T(8,128)(2,1)S(1)}, bf16[96,1024]{1,0:T(8,128)(2,1)S(1)}, u32[]{:S(2)}, u32[]{:S(2)}) %collective-permute-start.7) | collective-permute-done | bytes 196640 | tf_op jit(solution)/shard_map/ppermute | solution.py:26
  50.7 1.5 %collective-permute-start.19 = (bf16[96,1024]{1,0:T(8,128)(2,1)S(1)}, bf16[96,1024]{1,0:T(8,128)(2,1)S(1)}, u32[]{:S(2)}, u32[]{:S(2)}) collective-permute-start(bf16[96,1024]{1,0:T(8,128)(2,1)S(1)} %collective-permute-done.17.refs_0_), channel_id=1, source_target_pairs={{0,2},{1,3},{2,0},{3,1},{4,6},{5,7},{6,4},{7,5},{8,10},{9,11},{10,... | collective-permute-start | bytes 589832 | tf_op jit(solution)/shard_map/ppermute | solution.py:26
  54.0 3.1 %expert.4 = (bf16[288,4096]{1,0:T(8,128)(2,1)S(1)}, bf16[288,1024]{1,0:T(8,128)(2,1)S(1)}, bf16[288,1024]{1,0:T(8,128)(2,1)S(1)}, bf16[288,256]{1,0:T(8,128)(2,1...) custom-call(s32[2]{0:T(128)S(1)} %pad_add_fusion.1.pos, ...), custom_call_target="tpu_custom_call" | custom-call | tf_op jit(solution)/shard_map/expert/pallas_call | solution.py:201
  57.7 3.8 %expert.3 = (bf16[288,4096]{1,0:T(8,128)(2,1)S(1)}, bf16[288,1024]{1,0:T(8,128)(2,1)S(1)}, bf16[288,1024]{1,0:T(8,128)(2,1)S(1)}, bf16[288,256]{1,0:T(8,128)(2,1...) custom-call(s32[2]{0:T(128)S(1)} %pad_add_fusion.1.pos, ...), custom_call_target="tpu_custom_call" | custom-call | tf_op jit(solution)/shard_map/expert/pallas_call | solution.py:201
  64.4 2.7 %expert.5 = (bf16[192,4096]{1,0:T(8,128)(2,1)S(1)}, bf16[192,1024]{1,0:T(8,128)(2,1)S(1)}, bf16[192,1024]{1,0:T(8,128)(2,1)S(1)}, bf16[192,256]{1,0:T(8,128)(2,1...) custom-call(s32[2]{0:T(128)S(1)} %pad_add_fusion.1.pos, ...), custom_call_target="tpu_custom_call" | custom-call | tf_op jit(solution)/shard_map/expert/pallas_call | solution.py:201
  67.4 5.0 %collective-permute-start.36 = (bf16[96,1024]{1,0:T(8,128)(2,1)S(1)}, bf16[96,1024]{1,0:T(8,128)(2,1)S(1)}, u32[]{:S(2)}, u32[]{:S(2)}) collective-permute-start(bf16[96,1024]{1,0:T(8,128)(2,1)S(1)} %join.8), channel_id=1, source_target_pairs={{0,16},{4,20},{8,24},{12,28},{16,0},{20,4},{24,8},{28,12},{1,17},{... | collective-permute-start | bytes 589832 | tf_op jit(solution)/shard_map/ppermute | solution.py:26
  73.2 1.6 %collective-permute-start.30 = (bf16[192,512]{1,0:T(8,128)(2,1)S(1)}, bf16[192,512]{1,0:T(8,128)(2,1)S(1)}, u32[]{:S(2)}, u32[]{:S(2)}) collective-permute-start(bf16[192,512]{1,0:T(8,128)(2,1)S(1)} %get-tuple-element.91), channel_id=1, source_target_pairs={{0,2},{1,3},{2,0},{3,1},{4,6},{5,7},{6,4},{7,5},{8,10},{9,11},{10,... | collective-permute-start | bytes 589832 | tf_op jit(solution)/shard_map/ppermute | solution.py:26
  75.5 6.7 %collective-permute-done.36.refs_3_ = bf16[96,1024]{1,0:T(8,128)(2,1)S(1)} collective-permute-done((bf16[96,1024]{1,0:T(8,128)(2,1)S(1)}, bf16[96,1024]{1,0:T(8,128)(2,1)S(1)}, u32[]{:S(2)}, u32[]{:S(2)}) %collective-permute-start.36) | collective-permute-done | bytes 196640 | tf_op jit(solution)/shard_map/ppermute | solution.py:26
  83.3 1.6 %collective-permute-start.37 = (bf16[256,512]{1,0:T(8,128)(2,1)S(1)}, bf16[256,512]{1,0:T(8,128)(2,1)S(1)}, u32[]{:S(2)}, u32[]{:S(2)}) collective-permute-start(bf16[256,512]{1,0:T(8,128)(2,1)S(1)} %get-tuple-element.100), channel_id=1, source_target_pairs={{0,2},{1,3},{2,0},{3,1},{4,6},{5,7},{6,4},{7,5},{8,10},{9,11},{10,... | collective-permute-start | bytes 786440 | tf_op jit(solution)/shard_map/ppermute | solution.py:26
  85.5 4.2 %collective-permute-start.32 = (bf16[96,512]{1,0:T(8,128)(2,1)S(1)}, bf16[96,512]{1,0:T(8,128)(2,1)S(1)}, u32[]{:S(2)}, u32[]{:S(2)}) collective-permute-start(bf16[96,512]{1,0:T(8,128)(2,1)S(1)} %get-tuple-element.93), channel_id=1, source_target_pairs={{0,28},{4,24},{8,20},{12,16},{16,12},{20,8},{24,4},{28,0},{1,29},{... | collective-permute-start | bytes 294920 | tf_op jit(solution)/shard_map/ppermute | solution.py:26
  89.8 1.7 %collective-permute-start.28 = (bf16[96,512]{1,0:T(8,128)(2,1)S(1)}, bf16[96,512]{1,0:T(8,128)(2,1)S(1)}, u32[]{:S(2)}, u32[]{:S(2)}) collective-permute-start(bf16[96,512]{1,0:T(8,128)(2,1)S(1)} %get-tuple-element.87), channel_id=1, source_target_pairs={{0,20},{4,16},{8,28},{12,24},{16,4},{20,0},{24,12},{28,8},{1,21},{... | collective-permute-start | bytes 294920 | tf_op jit(solution)/shard_map/ppermute | solution.py:26
  92.4 2.5 %collective-permute-done.32.refs_3_ = bf16[96,512]{1,0:T(8,128)(2,1)S(1)} collective-permute-done((bf16[96,512]{1,0:T(8,128)(2,1)S(1)}, bf16[96,512]{1,0:T(8,128)(2,1)S(1)}, u32[]{:S(2)}, u32[]{:S(2)}) %collective-permute-start.32) | collective-permute-done | bytes 98336 | tf_op jit(solution)/shard_map/ppermute | solution.py:26
  96.0 3.9 %collective-permute-done.28.refs_1_ = bf16[96,512]{1,0:T(8,128)(2,1)S(1)} collective-permute-done((bf16[96,512]{1,0:T(8,128)(2,1)S(1)}, bf16[96,512]{1,0:T(8,128)(2,1)S(1)}, u32[]{:S(2)}, u32[]{:S(2)}) %collective-permute-start.28) | collective-permute-done | bytes 98336 | tf_op jit(solution)/shard_map/ppermute | solution.py:26
  100.8 5.9 %collective-permute-done.38.far = bf16[256,512]{1,0:T(8,128)(2,1)S(1)} collective-permute-done((bf16[256,512]{1,0:T(8,128)(2,1)S(1)}, bf16[256,512]{1,0:T(8,128)(2,1)S(1)}, u32[]{:S(2)}, u32[]{:S(2)}) %collective-permute-start.38) | collective-permute-done | bytes 262176 | tf_op jit(solution)/shard_map/ppermute | solution.py:26
  106.7 1.5 %collective-permute-done.40.mate_far = bf16[256,512]{1,0:T(8,128)(2,1)S(1)} collective-permute-done((bf16[256,512]{1,0:T(8,128)(2,1)S(1)}, bf16[256,512]{1,0:T(8,128)(2,1)S(1)}, u32[]{:S(2)}, u32[]{:S(2)}) %collective-permute-start.40) | collective-permute-done | bytes 262176 | tf_op jit(solution)/shard_map/ppermute | solution.py:26
  111.9 6.1 %weights.1 = (bf16[2048,256]{1,0:T(8,128)(2,1)}, bf16[2048,256]{1,0:T(8,128)(2,1)}, bf16[256,2048]{1,0:T(8,128)(2,1)}) custom-call(bf16[288,4096]{1,0:T(8,128)(2,1)S(1)} %get-tuple-element.60.refs_0_, bf16[288,256]{1,0:T(8,128)(2,1)S(1)} %get-tuple-element.61.refs_1_, bf16[288,256]{1,0:T(8,128)(2,1)S(1)} %get-tuple-element.62.refs_2_, ...), custom_call_target="tpu_custom_call" | custom-call | tf_op jit(solution)/shard_map/weights/pallas_call | solution.py:235
  118.0 2.6 %collective-permute-start.41 = (bf16[512,256]{1,0:T(8,128)(2,1)S(1)}, bf16[512,256]{1,0:T(8,128)(2,1)S(1)}, u32[]{:S(2)}, u32[]{:S(2)}) collective-permute-start(bf16[512,256]{1,0:T(8,128)(2,1)S(1)} %get-tuple-element.102), channel_id=1, source_target_pairs={{0,4},{4,0},{8,12},{12,8},{16,20},{20,16},{24,28},{28,24},{1,5},{5... | collective-permute-start | bytes 786440 | tf_op jit(solution)/shard_map/ppermute | solution.py:26
  122.9 10.3 %collective-permute-done.48 = f32[30,256]{1,0:T(8,128)S(1)} collective-permute-done((f32[30,256]{1,0:T(8,128)S(1)}, f32[30,256]{1,0:T(8,128)S(1)}, u32[]{:S(2)}, u32[]{:S(2)}) %collective-permute-start.48) | collective-permute-done | bytes 30752 | tf_op jit(solution)/shard_map/ppermute | solution.py:32
  133.6 2.3 %collective-permute-start.44 = (bf16[256,256]{1,0:T(8,128)(2,1)S(1)}, bf16[256,256]{1,0:T(8,128)(2,1)S(1)}, u32[]{:S(2)}, u32[]{:S(2)}) collective-permute-start(bf16[256,256]{1,0:T(8,128)(2,1)S(1)} %get-tuple-element.105), channel_id=1, source_target_pairs={{0,16},{4,20},{8,24},{12,28},{16,0},{20,4},{24,8},{28,12},{1,17},{... | collective-permute-start | bytes 393224 | tf_op jit(solution)/shard_map/ppermute | solution.py:26
  135.9 2.1 %collective-permute-start.45 = (bf16[256,256]{1,0:T(8,128)(2,1)S(1)}, bf16[256,256]{1,0:T(8,128)(2,1)S(1)}, u32[]{:S(2)}, u32[]{:S(2)}) collective-permute-start(bf16[256,256]{1,0:T(8,128)(2,1)S(1)} %get-tuple-element.106), channel_id=1, source_target_pairs={{0,24},{4,28},{8,16},{12,20},{16,8},{20,12},{24,0},{28,4},{1,25},{... | collective-permute-start | bytes 393224 | tf_op jit(solution)/shard_map/ppermute | solution.py:26
  139.9 6.4 %collective-permute-done.44 = bf16[256,256]{1,0:T(8,128)(2,1)S(1)} collective-permute-done((bf16[256,256]{1,0:T(8,128)(2,1)S(1)}, bf16[256,256]{1,0:T(8,128)(2,1)S(1)}, u32[]{:S(2)}, u32[]{:S(2)}) %collective-permute-start.44) | collective-permute-done | bytes 131104 | tf_op jit(solution)/shard_map/ppermute | solution.py:26
  (119 shorter events, 26.4 us)
Async XLA Ops:
  3.4 11.8 %collective-permute-start.9 = (bf16[96,1024]{1,0:T(8,128)(2,1)S(1)}, bf16[96,1024]{1,0:T(8,128)(2,1)S(1)}, u32[]{:S(2)}, u32[]{:S(2)}) collective-permute-start(bf16[96,1024]{1,0:T(8,128)(2,1)S(1)} %get-tuple-element.65), channel_id=1, source_target_pairs={{0,12},{4,8},{8,4},{12,0},{16,28},{20,24},{24,20},{28,16},{1,13},{... | collective-permute-start | bytes 589832 | tf_op jit(solution)/shard_map/ppermute | solution.py:26
  7.5 26.4 %collective-permute-start.13 = (bf16[96,1024]{1,0:T(8,128)(2,1)S(1)}, bf16[96,1024]{1,0:T(8,128)(2,1)S(1)}, u32[]{:S(2)}, u32[]{:S(2)}) collective-permute-start(bf16[96,1024]{1,0:T(8,128)(2,1)S(1)} %get-tuple-element.66), channel_id=1, source_target_pairs={{0,20},{4,16},{8,28},{12,24},{16,4},{20,0},{24,12},{28,8},{1,21},{... | collective-permute-start | bytes 589832 | tf_op jit(solution)/shard_map/ppermute | solution.py:26
  10.0 27.2 %collective-permute-start.5 = (bf16[96,1024]{1,0:T(8,128)(2,1)S(1)}, bf16[96,1024]{1,0:T(8,128)(2,1)S(1)}, u32[]{:S(2)}, u32[]{:S(2)}) collective-permute-start(bf16[96,1024]{1,0:T(8,128)(2,1)S(1)} %get-tuple-element.64), channel_id=1, source_target_pairs={{0,16},{4,20},{8,24},{12,28},{16,0},{20,4},{24,8},{28,12},{1,17},{... | collective-permute-start | bytes 589832 | tf_op jit(solution)/shard_map/ppermute | solution.py:26
  10.4 28.3 %collective-permute-start.17 = (bf16[96,1024]{1,0:T(8,128)(2,1)S(1)}, bf16[96,1024]{1,0:T(8,128)(2,1)S(1)}, u32[]{:S(2)}, u32[]{:S(2)}) collective-permute-start(bf16[96,1024]{1,0:T(8,128)(2,1)S(1)} %get-tuple-element.71), channel_id=1, source_target_pairs={{0,24},{4,28},{8,16},{12,20},{16,8},{20,12},{24,0},{28,4},{1,25},{... | collective-permute-start | bytes 589832 | tf_op jit(solution)/shard_map/ppermute | solution.py:26
  12.8 29.1 %collective-permute-start.21 = (bf16[96,1024]{1,0:T(8,128)(2,1)S(1)}, bf16[96,1024]{1,0:T(8,128)(2,1)S(1)}, u32[]{:S(2)}, u32[]{:S(2)}) collective-permute-start(bf16[96,1024]{1,0:T(8,128)(2,1)S(1)} %get-tuple-element.72), channel_id=1, source_target_pairs={{0,28},{4,24},{8,20},{12,16},{16,12},{20,8},{24,4},{28,0},{1,29},{... | collective-permute-start | bytes 589832 | tf_op jit(solution)/shard_map/ppermute | solution.py:26
  15.2 28.3 %collective-permute-start.11 = (bf16[96,1024]{1,0:T(8,128)(2,1)S(1)}, bf16[96,1024]{1,0:T(8,128)(2,1)S(1)}, u32[]{:S(2)}, u32[]{:S(2)}) collective-permute-start(bf16[96,1024]{1,0:T(8,128)(2,1)S(1)} %collective-permute-done.9.refs_4_), channel_id=1, source_target_pairs={{0,2},{1,3},{2,0},{3,1},{4,6},{5,7},{6,4},{7,5},{8,10},{9,11},{10,... | collective-permute-start | bytes 589832 | tf_op jit(solution)/shard_map/ppermute | solution.py:26
  33.9 9.6 %collective-permute-start.15 = (bf16[96,1024]{1,0:T(8,128)(2,1)S(1)}, bf16[96,1024]{1,0:T(8,128)(2,1)S(1)}, u32[]{:S(2)}, u32[]{:S(2)}) collective-permute-start(bf16[96,1024]{1,0:T(8,128)(2,1)S(1)} %collective-permute-done.13.refs_8_), channel_id=1, source_target_pairs={{0,2},{1,3},{2,0},{3,1},{4,6},{5,7},{6,4},{7,5},{8,10},{9,11},{10,... | collective-permute-start | bytes 589832 | tf_op jit(solution)/shard_map/ppermute | solution.py:26
  37.2 11.0 %collective-permute-start.1 = (bf16[96,2048]{1,0:T(8,128)(2,1)S(1)}, bf16[96,2048]{1,0:T(8,128)(2,1)S(1)}, u32[]{:S(2)}, u32[]{:S(2)}) collective-permute-start(bf16[96,2048]{1,0:T(8,128)(2,1)S(1)} %get-tuple-element.58), channel_id=1, source_target_pairs={{0,4},{4,0},{8,12},{12,8},{16,20},{20,16},{24,28},{28,24},{1,5},{5... | collective-permute-start | bytes 1179656 | tf_op jit(solution)/shard_map/ppermute | solution.py:26
  38.7 9.9 %collective-permute-start.3 = (bf16[96,2048]{1,0:T(8,128)(2,1)S(1)}, bf16[96,2048]{1,0:T(8,128)(2,1)S(1)}, u32[]{:S(2)}, u32[]{:S(2)}) collective-permute-start(bf16[96,2048]{1,0:T(8,128)(2,1)S(1)} %get-tuple-element.59), channel_id=1, source_target_pairs={{0,8},{4,12},{8,0},{12,4},{16,24},{20,28},{24,16},{28,20},{1,9},{5... | collective-permute-start | bytes 1179656 | tf_op jit(solution)/shard_map/ppermute | solution.py:26
  48.1 9.0 %collective-permute-start.2 = (bf16[96,2048]{1,0:T(8,128)(2,1)S(1)}, bf16[96,2048]{1,0:T(8,128)(2,1)S(1)}, u32[]{:S(2)}, u32[]{:S(2)}) collective-permute-start(bf16[96,2048]{1,0:T(8,128)(2,1)S(1)} %collective-permute-done.1.refs_2_), channel_id=1, source_target_pairs={{0,1},{1,0},{2,3},{3,2},{4,5},{5,4},{6,7},{7,6},{8,9},{9,8},{10,11... | collective-permute-start | bytes 1179656 | tf_op jit(solution)/shard_map/ppermute | solution.py:26
  48.6 9.1 %collective-permute-start.4 = (bf16[96,2048]{1,0:T(8,128)(2,1)S(1)}, bf16[96,2048]{1,0:T(8,128)(2,1)S(1)}, u32[]{:S(2)}, u32[]{:S(2)}) collective-permute-start(bf16[96,2048]{1,0:T(8,128)(2,1)S(1)} %collective-permute-done.3.refs_4_), channel_id=1, source_target_pairs={{0,1},{1,0},{2,3},{3,2},{4,5},{5,4},{6,7},{7,6},{8,9},{9,8},{10,11... | collective-permute-start | bytes 1179656 | tf_op jit(solution)/shard_map/ppermute | solution.py:26
  50.7 10.8 %collective-permute-start.19 = (bf16[96,1024]{1,0:T(8,128)(2,1)S(1)}, bf16[96,1024]{1,0:T(8,128)(2,1)S(1)}, u32[]{:S(2)}, u32[]{:S(2)}) collective-permute-start(bf16[96,1024]{1,0:T(8,128)(2,1)S(1)} %collective-permute-done.17.refs_0_), channel_id=1, source_target_pairs={{0,2},{1,3},{2,0},{3,1},{4,6},{5,7},{6,4},{7,5},{8,10},{9,11},{10,... | collective-permute-start | bytes 589832 | tf_op jit(solution)/shard_map/ppermute | solution.py:26
  52.3 9.8 %collective-permute-start.23 = (bf16[96,1024]{1,0:T(8,128)(2,1)S(1)}, bf16[96,1024]{1,0:T(8,128)(2,1)S(1)}, u32[]{:S(2)}, u32[]{:S(2)}) collective-permute-start(bf16[96,1024]{1,0:T(8,128)(2,1)S(1)} %collective-permute-done.21.refs_4_), channel_id=1, source_target_pairs={{0,2},{1,3},{2,0},{3,1},{4,6},{5,7},{6,4},{7,5},{8,10},{9,11},{10,... | collective-permute-start | bytes 589832 | tf_op jit(solution)/shard_map/ppermute | solution.py:26
  52.8 9.4 %collective-permute-start.18 = (bf16[96,1024]{1,0:T(8,128)(2,1)S(1)}, bf16[96,1024]{1,0:T(8,128)(2,1)S(1)}, u32[]{:S(2)}, u32[]{:S(2)}) collective-permute-start(bf16[96,1024]{1,0:T(8,128)(2,1)S(1)} %collective-permute-done.17.refs_0_), channel_id=1, source_target_pairs={{0,1},{1,0},{2,3},{3,2},{4,5},{5,4},{6,7},{7,6},{8,9},{9,8},{10,11... | collective-permute-start | bytes 589832 | tf_op jit(solution)/shard_map/ppermute | solution.py:26
  57.2 10.2 %collective-permute-start.25 = (bf16[288,1024]{1,0:T(8,128)(2,1)S(1)}, bf16[288,1024]{1,0:T(8,128)(2,1)S(1)}, u32[]{:S(2)}, u32[]{:S(2)}) collective-permute-start(bf16[288,1024]{1,0:T(8,128)(2,1)S(1)} %get-tuple-element.83), channel_id=1, source_target_pairs={{0,1},{1,0},{2,3},{3,2},{4,5},{5,4},{6,7},{7,6},{8,9},{9,8},{10,11... | collective-permute-start | bytes 1769480 | tf_op jit(solution)/shard_map/ppermute | solution.py:26
  61.5 10.9 %collective-permute-start.33 = (bf16[288,1024]{1,0:T(8,128)(2,1)S(1)}, bf16[288,1024]{1,0:T(8,128)(2,1)S(1)}, u32[]{:S(2)}, u32[]{:S(2)}) collective-permute-start(bf16[288,1024]{1,0:T(8,128)(2,1)S(1)} %get-tuple-element.95), channel_id=1, source_target_pairs={{0,1},{1,0},{2,3},{3,2},{4,5},{5,4},{6,7},{7,6},{8,9},{9,8},{10,11... | collective-permute-start | bytes 1769480 | tf_op jit(solution)/shard_map/ppermute | solution.py:26
  67.4 14.7 %collective-permute-start.36 = (bf16[96,1024]{1,0:T(8,128)(2,1)S(1)}, bf16[96,1024]{1,0:T(8,128)(2,1)S(1)}, u32[]{:S(2)}, u32[]{:S(2)}) collective-permute-start(bf16[96,1024]{1,0:T(8,128)(2,1)S(1)} %join.8), channel_id=1, source_target_pairs={{0,16},{4,20},{8,24},{12,28},{16,0},{20,4},{24,8},{28,12},{1,17},{... | collective-permute-start | bytes 589832 | tf_op jit(solution)/shard_map/ppermute | solution.py:26
  72.5 9.6 %collective-permute-start.34 = (bf16[96,1024]{1,0:T(8,128)(2,1)S(1)}, bf16[96,1024]{1,0:T(8,128)(2,1)S(1)}, u32[]{:S(2)}, u32[]{:S(2)}) collective-permute-start(bf16[96,1024]{1,0:T(8,128)(2,1)S(1)} %get-tuple-element.97), channel_id=1, source_target_pairs={{0,4},{4,0},{8,12},{12,8},{16,20},{20,16},{24,28},{28,24},{1,5},{5... | collective-permute-start | bytes 589832 | tf_op jit(solution)/shard_map/ppermute | solution.py:26
  73.1 9.7 %collective-permute-start.35 = (bf16[96,1024]{1,0:T(8,128)(2,1)S(1)}, bf16[96,1024]{1,0:T(8,128)(2,1)S(1)}, u32[]{:S(2)}, u32[]{:S(2)}) collective-permute-start(bf16[96,1024]{1,0:T(8,128)(2,1)S(1)} %get-tuple-element.98), channel_id=1, source_target_pairs={{0,8},{4,12},{8,0},{12,4},{16,24},{20,28},{24,16},{28,20},{1,9},{5... | collective-permute-start | bytes 589832 | tf_op jit(solution)/shard_map/ppermute | solution.py:26
  73.2 11.6 %collective-permute-start.30 = (bf16[192,512]{1,0:T(8,128)(2,1)S(1)}, bf16[192,512]{1,0:T(8,128)(2,1)S(1)}, u32[]{:S(2)}, u32[]{:S(2)}) collective-permute-start(bf16[192,512]{1,0:T(8,128)(2,1)S(1)} %get-tuple-element.91), channel_id=1, source_target_pairs={{0,2},{1,3},{2,0},{3,1},{4,6},{5,7},{6,4},{7,5},{8,10},{9,11},{10,... | collective-permute-start | bytes 589832 | tf_op jit(solution)/shard_map/ppermute | solution.py:26
  74.9 14.8 %collective-permute-start.26 = (bf16[192,512]{1,0:T(8,128)(2,1)S(1)}, bf16[192,512]{1,0:T(8,128)(2,1)S(1)}, u32[]{:S(2)}, u32[]{:S(2)}) collective-permute-start(bf16[192,512]{1,0:T(8,128)(2,1)S(1)} %get-tuple-element.85), channel_id=1, source_target_pairs={{0,2},{1,3},{2,0},{3,1},{4,6},{5,7},{6,4},{7,5},{8,10},{9,11},{10,... | collective-permute-start | bytes 589832 | tf_op jit(solution)/shard_map/ppermute | solution.py:26
  83.3 16.6 %collective-permute-start.37 = (bf16[256,512]{1,0:T(8,128)(2,1)S(1)}, bf16[256,512]{1,0:T(8,128)(2,1)S(1)}, u32[]{:S(2)}, u32[]{:S(2)}) collective-permute-start(bf16[256,512]{1,0:T(8,128)(2,1)S(1)} %get-tuple-element.100), channel_id=1, source_target_pairs={{0,2},{1,3},{2,0},{3,1},{4,6},{5,7},{6,4},{7,5},{8,10},{9,11},{10,... | collective-permute-start | bytes 786440 | tf_op jit(solution)/shard_map/ppermute | solution.py:26
  84.9 7.5 %collective-permute-start.31 = (bf16[96,512]{1,0:T(8,128)(2,1)S(1)}, bf16[96,512]{1,0:T(8,128)(2,1)S(1)}, u32[]{:S(2)}, u32[]{:S(2)}) collective-permute-start(bf16[96,512]{1,0:T(8,128)(2,1)S(1)} %get-tuple-element.92), channel_id=1, source_target_pairs={{0,24},{4,28},{8,16},{12,20},{16,8},{20,12},{24,0},{28,4},{1,25},{... | collective-permute-start | bytes 294920 | tf_op jit(solution)/shard_map/ppermute | solution.py:26
  85.5 9.4 %collective-permute-start.32 = (bf16[96,512]{1,0:T(8,128)(2,1)S(1)}, bf16[96,512]{1,0:T(8,128)(2,1)S(1)}, u32[]{:S(2)}, u32[]{:S(2)}) collective-permute-start(bf16[96,512]{1,0:T(8,128)(2,1)S(1)} %get-tuple-element.93), channel_id=1, source_target_pairs={{0,28},{4,24},{8,20},{12,16},{16,12},{20,8},{24,4},{28,0},{1,29},{... | collective-permute-start | bytes 294920 | tf_op jit(solution)/shard_map/ppermute | solution.py:26
  89.8 10.1 %collective-permute-start.28 = (bf16[96,512]{1,0:T(8,128)(2,1)S(1)}, bf16[96,512]{1,0:T(8,128)(2,1)S(1)}, u32[]{:S(2)}, u32[]{:S(2)}) collective-permute-start(bf16[96,512]{1,0:T(8,128)(2,1)S(1)} %get-tuple-element.87), channel_id=1, source_target_pairs={{0,20},{4,16},{8,28},{12,24},{16,4},{20,0},{24,12},{28,8},{1,21},{... | collective-permute-start | bytes 294920 | tf_op jit(solution)/shard_map/ppermute | solution.py:26
  111.4 9.3 %collective-permute-start.47 = (f32[2,256]{1,0:T(2,128)S(1)}, f32[2,256]{1,0:T(2,128)S(1)}, u32[]{:S(2)}, u32[]{:S(2)}) collective-permute-start(f32[2,256]{1,0:T(2,128)S(1)} %fusion.130), channel_id=1, source_target_pairs={{0,2},{1,3},{2,0},{3,1},{4,6},{5,7},{6,4},{7,5},{8,10},{9,11},{10,... | collective-permute-start | bytes 6152 | tf_op jit(solution)/shard_map/ppermute | solution.py:26
  118.0 15.4 %collective-permute-start.41 = (bf16[512,256]{1,0:T(8,128)(2,1)S(1)}, bf16[512,256]{1,0:T(8,128)(2,1)S(1)}, u32[]{:S(2)}, u32[]{:S(2)}) collective-permute-start(bf16[512,256]{1,0:T(8,128)(2,1)S(1)} %get-tuple-element.102), channel_id=1, source_target_pairs={{0,4},{4,0},{8,12},{12,8},{16,20},{20,16},{24,28},{28,24},{1,5},{5... | collective-permute-start | bytes 786440 | tf_op jit(solution)/shard_map/ppermute | solution.py:26
  120.6 12.9 %collective-permute-start.43 = (bf16[512,256]{1,0:T(8,128)(2,1)S(1)}, bf16[512,256]{1,0:T(8,128)(2,1)S(1)}, u32[]{:S(2)}, u32[]{:S(2)}) collective-permute-start(bf16[512,256]{1,0:T(8,128)(2,1)S(1)} %get-tuple-element.104), channel_id=1, source_target_pairs={{0,4},{4,0},{8,12},{12,8},{16,20},{20,16},{24,28},{28,24},{1,5},{5... | collective-permute-start | bytes 786440 | tf_op jit(solution)/shard_map/ppermute | solution.py:26
  120.9 12.4 %collective-permute-start.48 = (f32[30,256]{1,0:T(8,128)S(1)}, f32[30,256]{1,0:T(8,128)S(1)}, u32[]{:S(2)}, u32[]{:S(2)}) collective-permute-start(f32[30,256]{1,0:T(8,128)S(1)} %slice.444), channel_id=1, source_target_pairs={{4,0},{8,4},{12,8},{16,12},{20,16},{24,20},{28,24},{5,1},{9,5},{13... | collective-permute-start | bytes 92168 | tf_op jit(solution)/shard_map/ppermute | solution.py:32
  133.4 6.5 %collective-permute-start.42 = (bf16[256,256]{1,0:T(8,128)(2,1)S(1)}, bf16[256,256]{1,0:T(8,128)(2,1)S(1)}, u32[]{:S(2)}, u32[]{:S(2)}) collective-permute-start(bf16[256,256]{1,0:T(8,128)(2,1)S(1)} %add_convert_fusion), channel_id=1, source_target_pairs={{0,8},{4,12},{8,0},{12,4},{16,24},{20,28},{24,16},{28,20},{1,9},{5... | collective-permute-start | bytes 393224 | tf_op jit(solution)/shard_map/ppermute | solution.py:26
  133.6 12.7 %collective-permute-start.44 = (bf16[256,256]{1,0:T(8,128)(2,1)S(1)}, bf16[256,256]{1,0:T(8,128)(2,1)S(1)}, u32[]{:S(2)}, u32[]{:S(2)}) collective-permute-start(bf16[256,256]{1,0:T(8,128)(2,1)S(1)} %get-tuple-element.105), channel_id=1, source_target_pairs={{0,16},{4,20},{8,24},{12,28},{16,0},{20,4},{24,8},{28,12},{1,17},{... | collective-permute-start | bytes 393224 | tf_op jit(solution)/shard_map/ppermute | solution.py:26
  135.9 10.4 %collective-permute-start.45 = (bf16[256,256]{1,0:T(8,128)(2,1)S(1)}, bf16[256,256]{1,0:T(8,128)(2,1)S(1)}, u32[]{:S(2)}, u32[]{:S(2)}) collective-permute-start(bf16[256,256]{1,0:T(8,128)(2,1)S(1)} %get-tuple-element.106), channel_id=1, source_target_pairs={{0,24},{4,28},{8,16},{12,20},{16,8},{20,12},{24,0},{28,4},{1,25},{... | collective-permute-start | bytes 393224 | tf_op jit(solution)/shard_map/ppermute | solution.py:26
  (28 other events, 429.8 us)
where the time goes:
time: 147 us
  waiting for transfers between devices  68 us (46%)
  starting transfers between devices  52.6 us (36%)
  Pallas kernels  20.9 us (14%)
  other arithmetic  2.73 us (2%)
    ppermute x48, waiting for transfers between devices, swapped(): return lax.ppermute(block, axis, [(i, i ^ mask) for i in range(count)])  57.6 us
    ppermute x48, starting transfers between devices, swapped(): return lax.ppermute(block, axis, [(i, i ^ mask) for i in range(count)])  51.3 us
    ppermute x1, waiting for transfers between devices, shifted(): return lax.ppermute(block, axis, route)  10.3 us
    pallas_call x3, Pallas kernels, expert_math(): pl.pallas_call(functools.partial(expert_kernel, layout, fetch), in_specs=...  9.6 us
    pallas_call x1, Pallas kernels, weight_math(): pl.pallas_call(functools.partial(weight_kernel, len(flat) // 4), in_specs...  6.06 us
  transfers between devices with their start and end apart: 49, of which 23 were waited for; matrix products, arithmetic and copies ran while one was open for 1% of the time, Pallas kernels for 11%

commit v1 on v0

--- a/solution.py
+++ b/solution.py
@@ -211,35 +211,55 @@
     )(pos, *blocks, wg, wu, *(in_hbm(wd) if fetch else [wd]))
 
 
-def weight_kernel(groups, *refs):
-    ins, (gate_grad, up_grad, down_grad) = refs[: 4 * groups], refs[4 * groups :]
-    model = gate_grad.shape[0]
-    hidden = gate_grad.shape[1]
+def gates_kernel(groups, *refs):
+    ins, (gate_grad, up_grad) = refs[: 3 * groups], refs[3 * groups :]
+    model, hidden = gate_grad.shape
     width = model // 4
     for at in range(0, model, width):
         gate = jnp.zeros((width, hidden), F32)
         up = jnp.zeros((width, hidden), F32)
-        down = jnp.zeros((hidden, width), F32)
         for i in range(groups):
-            both, gd, ud, ha = ins[4 * i : 4 * i + 4]
+            both, gd, ud = ins[3 * i : 3 * i + 3]
             part = both[:, at : at + width]
             gate = gate + dot(part, gd[...], (0, 0))
             up = up + dot(part, ud[...], (0, 0))
-            down = down + dot(ha[...], both[:, model + at : model + at + width], (0, 0))
         gate_grad[at : at + width, :] = gate.astype(BF16)
         up_grad[at : at + width, :] = up.astype(BF16)
+
+
+def downs_kernel(groups, *refs):
+    ins, down_grad = refs[: 2 * groups], refs[2 * groups]
+    hidden, model = down_grad.shape
+    width = model // 4
+    for at in range(0, model, width):
+        down = jnp.zeros((hidden, width), F32)
+        for i in range(groups):
+            both, ha = ins[2 * i : 2 * i + 2]
+            down = down + dot(ha[...], both[:, model + at : model + at + width], (0, 0))
         down_grad[:, at : at + width] = down.astype(BF16)
 
 
 def weight_math(flat, model, hidden):
-    return pl.pallas_call(
-        functools.partial(weight_kernel, len(flat) // 4),
-        in_specs=[VMEM] * len(flat),
-        out_specs=[VMEM] * 3,
-        out_shape=[array(model, hidden), array(model, hidden), array(hidden, model)],
+    groups = [flat[i : i + 4] for i in range(0, len(flat), 4)]
+    gates_in = [a for both, gd, ud, ha in groups for a in (both, gd, ud)]
+    downs_in = [a for both, gd, ud, ha in groups for a in (both, ha)]
+    gate_grad, up_grad = pl.pallas_call(
+        functools.partial(gates_kernel, len(groups)),
+        in_specs=[VMEM] * len(gates_in),
+        out_specs=[VMEM] * 2,
+        out_shape=[array(model, hidden)] * 2,
         compiler_params=params(20),
-        name="weights",
-    )(*flat)
+        name="gates",
+    )(*gates_in)
+    down_grad = pl.pallas_call(
+        functools.partial(downs_kernel, len(groups)),
+        in_specs=[VMEM] * len(downs_in),
+        out_specs=VMEM,
+        out_shape=array(hidden, model),
+        compiler_params=params(20),
+        name="downs",
+    )(*downs_in)
+    return gate_grad, up_grad, down_grad
 
 
 def join_kernel(keep, mate, *outs):

time: 147 us -> 148 us (level)
    pallas_call x1 -> x2, Pallas kernels: 6.06 us -> 6.97 us  [the longest x1 4.23 us: weight_math(): pl.pallas_call(functools.partial(gates_kernel, len(groups)), in_specs=[VM...]
  transfers between devices with their start and end apart: 49 -> 49, of which waited for: 23 -> 23; matrix products, arithmetic and copies ran while one was open for 1% -> 1% of each run, Pallas kernels for 11% -> 12%
where the time goes in v1:
time: 148 us
  waiting for transfers between devices  68 us (46%)
  starting transfers between devices  52.6 us (36%)
  Pallas kernels  21.8 us (15%)
  other arithmetic  2.75 us (2%)
    ppermute x48, waiting for transfers between devices, swapped(): return lax.ppermute(block, axis, [(i, i ^ mask) for i in range(count)])  57.6 us
    ppermute x48, starting transfers between devices, swapped(): return lax.ppermute(block, axis, [(i, i ^ mask) for i in range(count)])  51.3 us
    ppermute x1, waiting for transfers between devices, shifted(): return lax.ppermute(block, axis, route)  10.3 us
    pallas_call x3, Pallas kernels, expert_math(): pl.pallas_call(functools.partial(expert_kernel, layout, fetch), in_specs=...  9.6 us
    pallas_call x1, Pallas kernels, weight_math(): pl.pallas_call(functools.partial(gates_kernel, len(groups)), in_specs=[VM...  4.23 us
  transfers between devices with their start and end apart: 49, of which 23 were waited for; matrix products, arithmetic and copies ran while one was open for 1% of the time, Pallas kernels for 12%

profile of v1, /device:TPU:0, one launch (start us, length us, event | category | flops | bytes accessed | tf_op | source)
XLA Modules:
  0.0 147.9 jit_solution(6095125892263104552)
XLA Ops:
  0.7 2.7 %dispatch.1 = (bf16[768,256]{1,0:T(8,128)(2,1)S(1)}, bf16[256,512]{1,0:T(8,128)(2,1)S(1)}, bf16[96,2048]{1,0:T(8,128)(2,1)S(1)}, bf16[96,2048]{1,0:T(8,128)(2,1)...) custom-call(s32[2]{0:T(128)S(1)} %pad_add_fusion.1.pos, ...), custom_call_target="tpu_custom_call" | custom-call | tf_op jit(solution)/shard_map/dispatch/pallas_call | solution.py:132
  3.4 4.0 %collective-permute-start.9 = (bf16[96,1024]{1,0:T(8,128)(2,1)S(1)}, bf16[96,1024]{1,0:T(8,128)(2,1)S(1)}, u32[]{:S(2)}, u32[]{:S(2)}) collective-permute-start(bf16[96,1024]{1,0:T(8,128)(2,1)S(1)} %get-tuple-element.63), channel_id=1, source_target_pairs={{0,12},{4,8},{8,4},{12,0},{16,28},{20,24},{24,20},{28,16},{1,13},{... | collective-permute-start | bytes 589832 | tf_op jit(solution)/shard_map/ppermute | solution.py:26
  7.5 2.6 %collective-permute-start.13 = (bf16[96,1024]{1,0:T(8,128)(2,1)S(1)}, bf16[96,1024]{1,0:T(8,128)(2,1)S(1)}, u32[]{:S(2)}, u32[]{:S(2)}) collective-permute-start(bf16[96,1024]{1,0:T(8,128)(2,1)S(1)} %get-tuple-element.64), channel_id=1, source_target_pairs={{0,20},{4,16},{8,28},{12,24},{16,4},{20,0},{24,12},{28,8},{1,21},{... | collective-permute-start | bytes 589832 | tf_op jit(solution)/shard_map/ppermute | solution.py:26
  10.4 2.5 %collective-permute-start.17 = (bf16[96,1024]{1,0:T(8,128)(2,1)S(1)}, bf16[96,1024]{1,0:T(8,128)(2,1)S(1)}, u32[]{:S(2)}, u32[]{:S(2)}) collective-permute-start(bf16[96,1024]{1,0:T(8,128)(2,1)S(1)} %get-tuple-element.68), channel_id=1, source_target_pairs={{0,24},{4,28},{8,16},{12,20},{16,8},{20,12},{24,0},{28,4},{1,25},{... | collective-permute-start | bytes 589832 | tf_op jit(solution)/shard_map/ppermute | solution.py:26
  12.8 2.3 %collective-permute-start.21 = (bf16[96,1024]{1,0:T(8,128)(2,1)S(1)}, bf16[96,1024]{1,0:T(8,128)(2,1)S(1)}, u32[]{:S(2)}, u32[]{:S(2)}) collective-permute-start(bf16[96,1024]{1,0:T(8,128)(2,1)S(1)} %get-tuple-element.69), channel_id=1, source_target_pairs={{0,28},{4,24},{8,20},{12,16},{16,12},{20,8},{24,4},{28,0},{1,29},{... | collective-permute-start | bytes 589832 | tf_op jit(solution)/shard_map/ppermute | solution.py:26
  15.2 1.8 %collective-permute-start.11 = (bf16[96,1024]{1,0:T(8,128)(2,1)S(1)}, bf16[96,1024]{1,0:T(8,128)(2,1)S(1)}, u32[]{:S(2)}, u32[]{:S(2)}) collective-permute-start(bf16[96,1024]{1,0:T(8,128)(2,1)S(1)} %collective-permute-done.9.refs_4_), channel_id=1, source_target_pairs={{0,2},{1,3},{2,0},{3,1},{4,6},{5,7},{6,4},{7,5},{8,10},{9,11},{10,... | collective-permute-start | bytes 589832 | tf_op jit(solution)/shard_map/ppermute | solution.py:26
  17.0 16.9 %collective-permute-done.13.refs_8_ = bf16[96,1024]{1,0:T(8,128)(2,1)S(1)} collective-permute-done((bf16[96,1024]{1,0:T(8,128)(2,1)S(1)}, bf16[96,1024]{1,0:T(8,128)(2,1)S(1)}, u32[]{:S(2)}, u32[]{:S(2)}) %collective-permute-start.13) | collective-permute-done | bytes 196640 | tf_op jit(solution)/shard_map/ppermute | solution.py:26
  33.9 1.5 %collective-permute-start.15 = (bf16[96,1024]{1,0:T(8,128)(2,1)S(1)}, bf16[96,1024]{1,0:T(8,128)(2,1)S(1)}, u32[]{:S(2)}, u32[]{:S(2)}) collective-permute-start(bf16[96,1024]{1,0:T(8,128)(2,1)S(1)} %collective-permute-done.13.refs_8_), channel_id=1, source_target_pairs={{0,2},{1,3},{2,0},{3,1},{4,6},{5,7},{6,4},{7,5},{8,10},{9,11},{10,... | collective-permute-start | bytes 589832 | tf_op jit(solution)/shard_map/ppermute | solution.py:26
  35.4 1.8 %collective-permute-done.5.refs_0_ = bf16[96,1024]{1,0:T(8,128)(2,1)S(1)} collective-permute-done((bf16[96,1024]{1,0:T(8,128)(2,1)S(1)}, bf16[96,1024]{1,0:T(8,128)(2,1)S(1)}, u32[]{:S(2)}, u32[]{:S(2)}) %collective-permute-start.5) | collective-permute-done | bytes 196640 | tf_op jit(solution)/shard_map/ppermute | solution.py:26
  38.7 3.3 %collective-permute-start.3 = (bf16[96,2048]{1,0:T(8,128)(2,1)S(1)}, bf16[96,2048]{1,0:T(8,128)(2,1)S(1)}, u32[]{:S(2)}, u32[]{:S(2)}) collective-permute-start(bf16[96,2048]{1,0:T(8,128)(2,1)S(1)} %get-tuple-element.58), channel_id=1, source_target_pairs={{0,8},{4,12},{8,0},{12,4},{16,24},{20,28},{24,16},{28,20},{1,9},{5... | collective-permute-start | bytes 1179656 | tf_op jit(solution)/shard_map/ppermute | solution.py:26
  41.9 1.5 %collective-permute-start.7 = (bf16[96,1024]{1,0:T(8,128)(2,1)S(1)}, bf16[96,1024]{1,0:T(8,128)(2,1)S(1)}, u32[]{:S(2)}, u32[]{:S(2)}) collective-permute-start(bf16[96,1024]{1,0:T(8,128)(2,1)S(1)} %collective-permute-done.5.refs_0_), channel_id=1, source_target_pairs={{0,2},{1,3},{2,0},{3,1},{4,6},{5,7},{6,4},{7,5},{8,10},{9,11},{10,... | collective-permute-start | bytes 589832 | tf_op jit(solution)/shard_map/ppermute | solution.py:26
  44.0 3.6 %collective-permute-done.7.refs_2_ = bf16[96,1024]{1,0:T(8,128)(2,1)S(1)} collective-permute-done((bf16[96,1024]{1,0:T(8,128)(2,1)S(1)}, bf16[96,1024]{1,0:T(8,128)(2,1)S(1)}, u32[]{:S(2)}, u32[]{:S(2)}) %collective-permute-start.7) | collective-permute-done | bytes 196640 | tf_op jit(solution)/shard_map/ppermute | solution.py:26
  50.7 1.5 %collective-permute-start.19 = (bf16[96,1024]{1,0:T(8,128)(2,1)S(1)}, bf16[96,1024]{1,0:T(8,128)(2,1)S(1)}, u32[]{:S(2)}, u32[]{:S(2)}) collective-permute-start(bf16[96,1024]{1,0:T(8,128)(2,1)S(1)} %collective-permute-done.17.refs_0_), channel_id=1, source_target_pairs={{0,2},{1,3},{2,0},{3,1},{4,6},{5,7},{6,4},{7,5},{8,10},{9,11},{10,... | collective-permute-start | bytes 589832 | tf_op jit(solution)/shard_map/ppermute | solution.py:26
  54.0 3.1 %expert.4 = (bf16[288,4096]{1,0:T(8,128)(2,1)S(1)}, bf16[288,1024]{1,0:T(8,128)(2,1)S(1)}, bf16[288,1024]{1,0:T(8,128)(2,1)S(1)}, bf16[288,256]{1,0:T(8,128)(2,1...) custom-call(s32[2]{0:T(128)S(1)} %pad_add_fusion.1.pos, ...), custom_call_target="tpu_custom_call" | custom-call | tf_op jit(solution)/shard_map/expert/pallas_call | solution.py:201
  57.7 3.8 %expert.3 = (bf16[288,4096]{1,0:T(8,128)(2,1)S(1)}, bf16[288,1024]{1,0:T(8,128)(2,1)S(1)}, bf16[288,1024]{1,0:T(8,128)(2,1)S(1)}, bf16[288,256]{1,0:T(8,128)(2,1...) custom-call(s32[2]{0:T(128)S(1)} %pad_add_fusion.1.pos, ...), custom_call_target="tpu_custom_call" | custom-call | tf_op jit(solution)/shard_map/expert/pallas_call | solution.py:201
  64.4 2.7 %expert.5 = (bf16[192,4096]{1,0:T(8,128)(2,1)S(1)}, bf16[192,1024]{1,0:T(8,128)(2,1)S(1)}, bf16[192,1024]{1,0:T(8,128)(2,1)S(1)}, bf16[192,256]{1,0:T(8,128)(2,1...) custom-call(s32[2]{0:T(128)S(1)} %pad_add_fusion.1.pos, ...), custom_call_target="tpu_custom_call" | custom-call | tf_op jit(solution)/shard_map/expert/pallas_call | solution.py:201
  67.4 5.0 %collective-permute-start.36 = (bf16[96,1024]{1,0:T(8,128)(2,1)S(1)}, bf16[96,1024]{1,0:T(8,128)(2,1)S(1)}, u32[]{:S(2)}, u32[]{:S(2)}) collective-permute-start(bf16[96,1024]{1,0:T(8,128)(2,1)S(1)} %join.8), channel_id=1, source_target_pairs={{0,16},{4,20},{8,24},{12,28},{16,0},{20,4},{24,8},{28,12},{1,17},{... | collective-permute-start | bytes 589832 | tf_op jit(solution)/shard_map/ppermute | solution.py:26
  73.2 1.6 %collective-permute-start.30 = (bf16[192,512]{1,0:T(8,128)(2,1)S(1)}, bf16[192,512]{1,0:T(8,128)(2,1)S(1)}, u32[]{:S(2)}, u32[]{:S(2)}) collective-permute-start(bf16[192,512]{1,0:T(8,128)(2,1)S(1)} %get-tuple-element.89), channel_id=1, source_target_pairs={{0,2},{1,3},{2,0},{3,1},{4,6},{5,7},{6,4},{7,5},{8,10},{9,11},{10,... | collective-permute-start | bytes 589832 | tf_op jit(solution)/shard_map/ppermute | solution.py:26
  75.5 6.7 %collective-permute-done.36.refs_3_ = bf16[96,1024]{1,0:T(8,128)(2,1)S(1)} collective-permute-done((bf16[96,1024]{1,0:T(8,128)(2,1)S(1)}, bf16[96,1024]{1,0:T(8,128)(2,1)S(1)}, u32[]{:S(2)}, u32[]{:S(2)}) %collective-permute-start.36) | collective-permute-done | bytes 196640 | tf_op jit(solution)/shard_map/ppermute | solution.py:26
  83.3 1.6 %collective-permute-start.37 = (bf16[256,512]{1,0:T(8,128)(2,1)S(1)}, bf16[256,512]{1,0:T(8,128)(2,1)S(1)}, u32[]{:S(2)}, u32[]{:S(2)}) collective-permute-start(bf16[256,512]{1,0:T(8,128)(2,1)S(1)} %get-tuple-element.98), channel_id=1, source_target_pairs={{0,2},{1,3},{2,0},{3,1},{4,6},{5,7},{6,4},{7,5},{8,10},{9,11},{10,... | collective-permute-start | bytes 786440 | tf_op jit(solution)/shard_map/ppermute | solution.py:26
  85.5 4.2 %collective-permute-start.32 = (bf16[96,512]{1,0:T(8,128)(2,1)S(1)}, bf16[96,512]{1,0:T(8,128)(2,1)S(1)}, u32[]{:S(2)}, u32[]{:S(2)}) collective-permute-start(bf16[96,512]{1,0:T(8,128)(2,1)S(1)} %get-tuple-element.91), channel_id=1, source_target_pairs={{0,28},{4,24},{8,20},{12,16},{16,12},{20,8},{24,4},{28,0},{1,29},{... | collective-permute-start | bytes 294920 | tf_op jit(solution)/shard_map/ppermute | solution.py:26
  89.8 1.7 %collective-permute-start.28 = (bf16[96,512]{1,0:T(8,128)(2,1)S(1)}, bf16[96,512]{1,0:T(8,128)(2,1)S(1)}, u32[]{:S(2)}, u32[]{:S(2)}) collective-permute-start(bf16[96,512]{1,0:T(8,128)(2,1)S(1)} %get-tuple-element.85), channel_id=1, source_target_pairs={{0,20},{4,16},{8,28},{12,24},{16,4},{20,0},{24,12},{28,8},{1,21},{... | collective-permute-start | bytes 294920 | tf_op jit(solution)/shard_map/ppermute | solution.py:26
  92.4 2.5 %collective-permute-done.32.refs_3_ = bf16[96,512]{1,0:T(8,128)(2,1)S(1)} collective-permute-done((bf16[96,512]{1,0:T(8,128)(2,1)S(1)}, bf16[96,512]{1,0:T(8,128)(2,1)S(1)}, u32[]{:S(2)}, u32[]{:S(2)}) %collective-permute-start.32) | collective-permute-done | bytes 98336 | tf_op jit(solution)/shard_map/ppermute | solution.py:26
  96.0 3.9 %collective-permute-done.28.refs_1_ = bf16[96,512]{1,0:T(8,128)(2,1)S(1)} collective-permute-done((bf16[96,512]{1,0:T(8,128)(2,1)S(1)}, bf16[96,512]{1,0:T(8,128)(2,1)S(1)}, u32[]{:S(2)}, u32[]{:S(2)}) %collective-permute-start.28) | collective-permute-done | bytes 98336 | tf_op jit(solution)/shard_map/ppermute | solution.py:26
  100.8 5.9 %collective-permute-done.38.far = bf16[256,512]{1,0:T(8,128)(2,1)S(1)} collective-permute-done((bf16[256,512]{1,0:T(8,128)(2,1)S(1)}, bf16[256,512]{1,0:T(8,128)(2,1)S(1)}, u32[]{:S(2)}, u32[]{:S(2)}) %collective-permute-start.38) | collective-permute-done | bytes 262176 | tf_op jit(solution)/shard_map/ppermute | solution.py:26
  111.9 2.7 %downs.1 = bf16[256,2048]{1,0:T(8,128)(2,1)} custom-call(bf16[288,4096]{1,0:T(8,128)(2,1)S(1)} %get-tuple-element.59.refs_0_, bf16[288,256]{1,0:T(8,128)(2,1)S(1)} %get-tuple-element.75.refs_1_, bf16[288,4096]{1,0:T(8,128)(2,1)S(1)} %get-tuple-element.65.refs_3_.refs_2_, bf16[288,256]{1,0:T(8,128)(2,1)S(1)} %get-tuple-element.76.refs_3_, ...), custom_call_target="tpu_custom_call" | custom-call | tf_op jit(solution)/shard_map/downs/pallas_call | solution.py:254
  114.7 4.2 %gates.1 = (bf16[2048,256]{1,0:T(8,128)(2,1)}, bf16[2048,256]{1,0:T(8,128)(2,1)}) custom-call(bf16[288,4096]{1,0:T(8,128)(2,1)S(1)} %get-tuple-element.59.refs_0_, bf16[288,256]{1,0:T(8,128)(2,1)S(1)} %get-tuple-element.60.refs_1_, bf16[288,256]{1,0:T(8,128)(2,1)S(1)} %get-tuple-element.61.refs_2_, bf16[288,4096]{1,0:T(8,128)(2,1)S(1)} %get-tuple-element.65.refs_3_.refs_2_, ...), custom_call_target="tpu_custom_call" | custom-call | tf_op jit(solution)/shard_map/gates/pallas_call | solution.py:246
  118.9 2.6 %collective-permute-start.41 = (bf16[512,256]{1,0:T(8,128)(2,1)S(1)}, bf16[512,256]{1,0:T(8,128)(2,1)S(1)}, u32[]{:S(2)}, u32[]{:S(2)}) collective-permute-start(bf16[512,256]{1,0:T(8,128)(2,1)S(1)} %get-tuple-element.100), channel_id=1, source_target_pairs={{0,4},{4,0},{8,12},{12,8},{16,20},{20,16},{24,28},{28,24},{1,5},{5... | collective-permute-start | bytes 786440 | tf_op jit(solution)/shard_map/ppermute | solution.py:26
  123.8 10.3 %collective-permute-done.48 = f32[30,256]{1,0:T(8,128)S(1)} collective-permute-done((f32[30,256]{1,0:T(8,128)S(1)}, f32[30,256]{1,0:T(8,128)S(1)}, u32[]{:S(2)}, u32[]{:S(2)}) %collective-permute-start.48) | collective-permute-done | bytes 30752 | tf_op jit(solution)/shard_map/ppermute | solution.py:32
  134.5 2.3 %collective-permute-start.44 = (bf16[256,256]{1,0:T(8,128)(2,1)S(1)}, bf16[256,256]{1,0:T(8,128)(2,1)S(1)}, u32[]{:S(2)}, u32[]{:S(2)}) collective-permute-start(bf16[256,256]{1,0:T(8,128)(2,1)S(1)} %get-tuple-element.103), channel_id=1, source_target_pairs={{0,16},{4,20},{8,24},{12,28},{16,0},{20,4},{24,8},{28,12},{1,17},{... | collective-permute-start | bytes 393224 | tf_op jit(solution)/shard_map/ppermute | solution.py:26
  136.8 2.1 %collective-permute-start.45 = (bf16[256,256]{1,0:T(8,128)(2,1)S(1)}, bf16[256,256]{1,0:T(8,128)(2,1)S(1)}, u32[]{:S(2)}, u32[]{:S(2)}) collective-permute-start(bf16[256,256]{1,0:T(8,128)(2,1)S(1)} %get-tuple-element.104), channel_id=1, source_target_pairs={{0,24},{4,28},{8,16},{12,20},{16,8},{20,12},{24,0},{28,4},{1,25},{... | collective-permute-start | bytes 393224 | tf_op jit(solution)/shard_map/ppermute | solution.py:26
  140.8 6.4 %collective-permute-done.44 = bf16[256,256]{1,0:T(8,128)(2,1)S(1)} collective-permute-done((bf16[256,256]{1,0:T(8,128)(2,1)S(1)}, bf16[256,256]{1,0:T(8,128)(2,1)S(1)}, u32[]{:S(2)}, u32[]{:S(2)}) %collective-permute-start.44) | collective-permute-done | bytes 131104 | tf_op jit(solution)/shard_map/ppermute | solution.py:26
  (120 shorter events, 27.9 us)
Async XLA Ops:
  3.4 11.8 %collective-permute-start.9 = (bf16[96,1024]{1,0:T(8,128)(2,1)S(1)}, bf16[96,1024]{1,0:T(8,128)(2,1)S(1)}, u32[]{:S(2)}, u32[]{:S(2)}) collective-permute-start(bf16[96,1024]{1,0:T(8,128)(2,1)S(1)} %get-tuple-element.63), channel_id=1, source_target_pairs={{0,12},{4,8},{8,4},{12,0},{16,28},{20,24},{24,20},{28,16},{1,13},{... | collective-permute-start | bytes 589832 | tf_op jit(solution)/shard_map/ppermute | solution.py:26
  7.5 26.4 %collective-permute-start.13 = (bf16[96,1024]{1,0:T(8,128)(2,1)S(1)}, bf16[96,1024]{1,0:T(8,128)(2,1)S(1)}, u32[]{:S(2)}, u32[]{:S(2)}) collective-permute-start(bf16[96,1024]{1,0:T(8,128)(2,1)S(1)} %get-tuple-element.64), channel_id=1, source_target_pairs={{0,20},{4,16},{8,28},{12,24},{16,4},{20,0},{24,12},{28,8},{1,21},{... | collective-permute-start | bytes 589832 | tf_op jit(solution)/shard_map/ppermute | solution.py:26
  10.0 27.2 %collective-permute-start.5 = (bf16[96,1024]{1,0:T(8,128)(2,1)S(1)}, bf16[96,1024]{1,0:T(8,128)(2,1)S(1)}, u32[]{:S(2)}, u32[]{:S(2)}) collective-permute-start(bf16[96,1024]{1,0:T(8,128)(2,1)S(1)} %get-tuple-element.62), channel_id=1, source_target_pairs={{0,16},{4,20},{8,24},{12,28},{16,0},{20,4},{24,8},{28,12},{1,17},{... | collective-permute-start | bytes 589832 | tf_op jit(solution)/shard_map/ppermute | solution.py:26
  10.4 28.3 %collective-permute-start.17 = (bf16[96,1024]{1,0:T(8,128)(2,1)S(1)}, bf16[96,1024]{1,0:T(8,128)(2,1)S(1)}, u32[]{:S(2)}, u32[]{:S(2)}) collective-permute-start(bf16[96,1024]{1,0:T(8,128)(2,1)S(1)} %get-tuple-element.68), channel_id=1, source_target_pairs={{0,24},{4,28},{8,16},{12,20},{16,8},{20,12},{24,0},{28,4},{1,25},{... | collective-permute-start | bytes 589832 | tf_op jit(solution)/shard_map/ppermute | solution.py:26
  12.8 29.1 %collective-permute-start.21 = (bf16[96,1024]{1,0:T(8,128)(2,1)S(1)}, bf16[96,1024]{1,0:T(8,128)(2,1)S(1)}, u32[]{:S(2)}, u32[]{:S(2)}) collective-permute-start(bf16[96,1024]{1,0:T(8,128)(2,1)S(1)} %get-tuple-element.69), channel_id=1, source_target_pairs={{0,28},{4,24},{8,20},{12,16},{16,12},{20,8},{24,4},{28,0},{1,29},{... | collective-permute-start | bytes 589832 | tf_op jit(solution)/shard_map/ppermute | solution.py:26
  15.2 28.3 %collective-permute-start.11 = (bf16[96,1024]{1,0:T(8,128)(2,1)S(1)}, bf16[96,1024]{1,0:T(8,128)(2,1)S(1)}, u32[]{:S(2)}, u32[]{:S(2)}) collective-permute-start(bf16[96,1024]{1,0:T(8,128)(2,1)S(1)} %collective-permute-done.9.refs_4_), channel_id=1, source_target_pairs={{0,2},{1,3},{2,0},{3,1},{4,6},{5,7},{6,4},{7,5},{8,10},{9,11},{10,... | collective-permute-start | bytes 589832 | tf_op jit(solution)/shard_map/ppermute | solution.py:26
  33.9 9.6 %collective-permute-start.15 = (bf16[96,1024]{1,0:T(8,128)(2,1)S(1)}, bf16[96,1024]{1,0:T(8,128)(2,1)S(1)}, u32[]{:S(2)}, u32[]{:S(2)}) collective-permute-start(bf16[96,1024]{1,0:T(8,128)(2,1)S(1)} %collective-permute-done.13.refs_8_), channel_id=1, source_target_pairs={{0,2},{1,3},{2,0},{3,1},{4,6},{5,7},{6,4},{7,5},{8,10},{9,11},{10,... | collective-permute-start | bytes 589832 | tf_op jit(solution)/shard_map/ppermute | solution.py:26
  37.2 11.0 %collective-permute-start.1 = (bf16[96,2048]{1,0:T(8,128)(2,1)S(1)}, bf16[96,2048]{1,0:T(8,128)(2,1)S(1)}, u32[]{:S(2)}, u32[]{:S(2)}) collective-permute-start(bf16[96,2048]{1,0:T(8,128)(2,1)S(1)} %get-tuple-element.57), channel_id=1, source_target_pairs={{0,4},{4,0},{8,12},{12,8},{16,20},{20,16},{24,28},{28,24},{1,5},{5... | collective-permute-start | bytes 1179656 | tf_op jit(solution)/shard_map/ppermute | solution.py:26
  38.7 9.9 %collective-permute-start.3 = (bf16[96,2048]{1,0:T(8,128)(2,1)S(1)}, bf16[96,2048]{1,0:T(8,128)(2,1)S(1)}, u32[]{:S(2)}, u32[]{:S(2)}) collective-permute-start(bf16[96,2048]{1,0:T(8,128)(2,1)S(1)} %get-tuple-element.58), channel_id=1, source_target_pairs={{0,8},{4,12},{8,0},{12,4},{16,24},{20,28},{24,16},{28,20},{1,9},{5... | collective-permute-start | bytes 1179656 | tf_op jit(solution)/shard_map/ppermute | solution.py:26
  48.1 9.0 %collective-permute-start.2 = (bf16[96,2048]{1,0:T(8,128)(2,1)S(1)}, bf16[96,2048]{1,0:T(8,128)(2,1)S(1)}, u32[]{:S(2)}, u32[]{:S(2)}) collective-permute-start(bf16[96,2048]{1,0:T(8,128)(2,1)S(1)} %collective-permute-done.1.refs_2_), channel_id=1, source_target_pairs={{0,1},{1,0},{2,3},{3,2},{4,5},{5,4},{6,7},{7,6},{8,9},{9,8},{10,11... | collective-permute-start | bytes 1179656 | tf_op jit(solution)/shard_map/ppermute | solution.py:26
  48.6 9.1 %collective-permute-start.4 = (bf16[96,2048]{1,0:T(8,128)(2,1)S(1)}, bf16[96,2048]{1,0:T(8,128)(2,1)S(1)}, u32[]{:S(2)}, u32[]{:S(2)}) collective-permute-start(bf16[96,2048]{1,0:T(8,128)(2,1)S(1)} %collective-permute-done.3.refs_4_), channel_id=1, source_target_pairs={{0,1},{1,0},{2,3},{3,2},{4,5},{5,4},{6,7},{7,6},{8,9},{9,8},{10,11... | collective-permute-start | bytes 1179656 | tf_op jit(solution)/shard_map/ppermute | solution.py:26
  50.7 10.8 %collective-permute-start.19 = (bf16[96,1024]{1,0:T(8,128)(2,1)S(1)}, bf16[96,1024]{1,0:T(8,128)(2,1)S(1)}, u32[]{:S(2)}, u32[]{:S(2)}) collective-permute-start(bf16[96,1024]{1,0:T(8,128)(2,1)S(1)} %collective-permute-done.17.refs_0_), channel_id=1, source_target_pairs={{0,2},{1,3},{2,0},{3,1},{4,6},{5,7},{6,4},{7,5},{8,10},{9,11},{10,... | collective-permute-start | bytes 589832 | tf_op jit(solution)/shard_map/ppermute | solution.py:26
  52.3 9.8 %collective-permute-start.23 = (bf16[96,1024]{1,0:T(8,128)(2,1)S(1)}, bf16[96,1024]{1,0:T(8,128)(2,1)S(1)}, u32[]{:S(2)}, u32[]{:S(2)}) collective-permute-start(bf16[96,1024]{1,0:T(8,128)(2,1)S(1)} %collective-permute-done.21.refs_4_), channel_id=1, source_target_pairs={{0,2},{1,3},{2,0},{3,1},{4,6},{5,7},{6,4},{7,5},{8,10},{9,11},{10,... | collective-permute-start | bytes 589832 | tf_op jit(solution)/shard_map/ppermute | solution.py:26
  52.8 9.4 %collective-permute-start.18 = (bf16[96,1024]{1,0:T(8,128)(2,1)S(1)}, bf16[96,1024]{1,0:T(8,128)(2,1)S(1)}, u32[]{:S(2)}, u32[]{:S(2)}) collective-permute-start(bf16[96,1024]{1,0:T(8,128)(2,1)S(1)} %collective-permute-done.17.refs_0_), channel_id=1, source_target_pairs={{0,1},{1,0},{2,3},{3,2},{4,5},{5,4},{6,7},{7,6},{8,9},{9,8},{10,11... | collective-permute-start | bytes 589832 | tf_op jit(solution)/shard_map/ppermute | solution.py:26
  57.2 10.2 %collective-permute-start.25 = (bf16[288,1024]{1,0:T(8,128)(2,1)S(1)}, bf16[288,1024]{1,0:T(8,128)(2,1)S(1)}, u32[]{:S(2)}, u32[]{:S(2)}) collective-permute-start(bf16[288,1024]{1,0:T(8,128)(2,1)S(1)} %get-tuple-element.81), channel_id=1, source_target_pairs={{0,1},{1,0},{2,3},{3,2},{4,5},{5,4},{6,7},{7,6},{8,9},{9,8},{10,11... | collective-permute-start | bytes 1769480 | tf_op jit(solution)/shard_map/ppermute | solution.py:26
  61.5 10.9 %collective-permute-start.33 = (bf16[288,1024]{1,0:T(8,128)(2,1)S(1)}, bf16[288,1024]{1,0:T(8,128)(2,1)S(1)}, u32[]{:S(2)}, u32[]{:S(2)}) collective-permute-start(bf16[288,1024]{1,0:T(8,128)(2,1)S(1)} %get-tuple-element.93), channel_id=1, source_target_pairs={{0,1},{1,0},{2,3},{3,2},{4,5},{5,4},{6,7},{7,6},{8,9},{9,8},{10,11... | collective-permute-start | bytes 1769480 | tf_op jit(solution)/shard_map/ppermute | solution.py:26
  67.4 14.7 %collective-permute-start.36 = (bf16[96,1024]{1,0:T(8,128)(2,1)S(1)}, bf16[96,1024]{1,0:T(8,128)(2,1)S(1)}, u32[]{:S(2)}, u32[]{:S(2)}) collective-permute-start(bf16[96,1024]{1,0:T(8,128)(2,1)S(1)} %join.8), channel_id=1, source_target_pairs={{0,16},{4,20},{8,24},{12,28},{16,0},{20,4},{24,8},{28,12},{1,17},{... | collective-permute-start | bytes 589832 | tf_op jit(solution)/shard_map/ppermute | solution.py:26
  72.5 9.6 %collective-permute-start.34 = (bf16[96,1024]{1,0:T(8,128)(2,1)S(1)}, bf16[96,1024]{1,0:T(8,128)(2,1)S(1)}, u32[]{:S(2)}, u32[]{:S(2)}) collective-permute-start(bf16[96,1024]{1,0:T(8,128)(2,1)S(1)} %get-tuple-element.95), channel_id=1, source_target_pairs={{0,4},{4,0},{8,12},{12,8},{16,20},{20,16},{24,28},{28,24},{1,5},{5... | collective-permute-start | bytes 589832 | tf_op jit(solution)/shard_map/ppermute | solution.py:26
  73.1 9.7 %collective-permute-start.35 = (bf16[96,1024]{1,0:T(8,128)(2,1)S(1)}, bf16[96,1024]{1,0:T(8,128)(2,1)S(1)}, u32[]{:S(2)}, u32[]{:S(2)}) collective-permute-start(bf16[96,1024]{1,0:T(8,128)(2,1)S(1)} %get-tuple-element.96), channel_id=1, source_target_pairs={{0,8},{4,12},{8,0},{12,4},{16,24},{20,28},{24,16},{28,20},{1,9},{5... | collective-permute-start | bytes 589832 | tf_op jit(solution)/shard_map/ppermute | solution.py:26
  73.2 11.6 %collective-permute-start.30 = (bf16[192,512]{1,0:T(8,128)(2,1)S(1)}, bf16[192,512]{1,0:T(8,128)(2,1)S(1)}, u32[]{:S(2)}, u32[]{:S(2)}) collective-permute-start(bf16[192,512]{1,0:T(8,128)(2,1)S(1)} %get-tuple-element.89), channel_id=1, source_target_pairs={{0,2},{1,3},{2,0},{3,1},{4,6},{5,7},{6,4},{7,5},{8,10},{9,11},{10,... | collective-permute-start | bytes 589832 | tf_op jit(solution)/shard_map/ppermute | solution.py:26
  74.9 14.8 %collective-permute-start.26 = (bf16[192,512]{1,0:T(8,128)(2,1)S(1)}, bf16[192,512]{1,0:T(8,128)(2,1)S(1)}, u32[]{:S(2)}, u32[]{:S(2)}) collective-permute-start(bf16[192,512]{1,0:T(8,128)(2,1)S(1)} %get-tuple-element.83), channel_id=1, source_target_pairs={{0,2},{1,3},{2,0},{3,1},{4,6},{5,7},{6,4},{7,5},{8,10},{9,11},{10,... | collective-permute-start | bytes 589832 | tf_op jit(solution)/shard_map/ppermute | solution.py:26
  83.3 16.6 %collective-permute-start.37 = (bf16[256,512]{1,0:T(8,128)(2,1)S(1)}, bf16[256,512]{1,0:T(8,128)(2,1)S(1)}, u32[]{:S(2)}, u32[]{:S(2)}) collective-permute-start(bf16[256,512]{1,0:T(8,128)(2,1)S(1)} %get-tuple-element.98), channel_id=1, source_target_pairs={{0,2},{1,3},{2,0},{3,1},{4,6},{5,7},{6,4},{7,5},{8,10},{9,11},{10,... | collective-permute-start | bytes 786440 | tf_op jit(solution)/shard_map/ppermute | solution.py:26
  84.9 7.5 %collective-permute-start.31 = (bf16[96,512]{1,0:T(8,128)(2,1)S(1)}, bf16[96,512]{1,0:T(8,128)(2,1)S(1)}, u32[]{:S(2)}, u32[]{:S(2)}) collective-permute-start(bf16[96,512]{1,0:T(8,128)(2,1)S(1)} %get-tuple-element.90), channel_id=1, source_target_pairs={{0,24},{4,28},{8,16},{12,20},{16,8},{20,12},{24,0},{28,4},{1,25},{... | collective-permute-start | bytes 294920 | tf_op jit(solution)/shard_map/ppermute | solution.py:26
  85.5 9.4 %collective-permute-start.32 = (bf16[96,512]{1,0:T(8,128)(2,1)S(1)}, bf16[96,512]{1,0:T(8,128)(2,1)S(1)}, u32[]{:S(2)}, u32[]{:S(2)}) collective-permute-start(bf16[96,512]{1,0:T(8,128)(2,1)S(1)} %get-tuple-element.91), channel_id=1, source_target_pairs={{0,28},{4,24},{8,20},{12,16},{16,12},{20,8},{24,4},{28,0},{1,29},{... | collective-permute-start | bytes 294920 | tf_op jit(solution)/shard_map/ppermute | solution.py:26
  89.8 10.1 %collective-permute-start.28 = (bf16[96,512]{1,0:T(8,128)(2,1)S(1)}, bf16[96,512]{1,0:T(8,128)(2,1)S(1)}, u32[]{:S(2)}, u32[]{:S(2)}) collective-permute-start(bf16[96,512]{1,0:T(8,128)(2,1)S(1)} %get-tuple-element.85), channel_id=1, source_target_pairs={{0,20},{4,16},{8,28},{12,24},{16,4},{20,0},{24,12},{28,8},{1,21},{... | collective-permute-start | bytes 294920 | tf_op jit(solution)/shard_map/ppermute | solution.py:26
  111.4 10.2 %collective-permute-start.47 = (f32[2,256]{1,0:T(2,128)S(1)}, f32[2,256]{1,0:T(2,128)S(1)}, u32[]{:S(2)}, u32[]{:S(2)}) collective-permute-start(f32[2,256]{1,0:T(2,128)S(1)} %fusion.130), channel_id=1, source_target_pairs={{0,2},{1,3},{2,0},{3,1},{4,6},{5,7},{6,4},{7,5},{8,10},{9,11},{10,... | collective-permute-start | bytes 6152 | tf_op jit(solution)/shard_map/ppermute | solution.py:26
  118.9 15.4 %collective-permute-start.41 = (bf16[512,256]{1,0:T(8,128)(2,1)S(1)}, bf16[512,256]{1,0:T(8,128)(2,1)S(1)}, u32[]{:S(2)}, u32[]{:S(2)}) collective-permute-start(bf16[512,256]{1,0:T(8,128)(2,1)S(1)} %get-tuple-element.100), channel_id=1, source_target_pairs={{0,4},{4,0},{8,12},{12,8},{16,20},{20,16},{24,28},{28,24},{1,5},{5... | collective-permute-start | bytes 786440 | tf_op jit(solution)/shard_map/ppermute | solution.py:26
  121.5 12.9 %collective-permute-start.43 = (bf16[512,256]{1,0:T(8,128)(2,1)S(1)}, bf16[512,256]{1,0:T(8,128)(2,1)S(1)}, u32[]{:S(2)}, u32[]{:S(2)}) collective-permute-start(bf16[512,256]{1,0:T(8,128)(2,1)S(1)} %get-tuple-element.102), channel_id=1, source_target_pairs={{0,4},{4,0},{8,12},{12,8},{16,20},{20,16},{24,28},{28,24},{1,5},{5... | collective-permute-start | bytes 786440 | tf_op jit(solution)/shard_map/ppermute | solution.py:26
  121.8 12.4 %collective-permute-start.48 = (f32[30,256]{1,0:T(8,128)S(1)}, f32[30,256]{1,0:T(8,128)S(1)}, u32[]{:S(2)}, u32[]{:S(2)}) collective-permute-start(f32[30,256]{1,0:T(8,128)S(1)} %slice.444), channel_id=1, source_target_pairs={{4,0},{8,4},{12,8},{16,12},{20,16},{24,20},{28,24},{5,1},{9,5},{13... | collective-permute-start | bytes 92168 | tf_op jit(solution)/shard_map/ppermute | solution.py:32
  134.3 6.5 %collective-permute-start.42 = (bf16[256,256]{1,0:T(8,128)(2,1)S(1)}, bf16[256,256]{1,0:T(8,128)(2,1)S(1)}, u32[]{:S(2)}, u32[]{:S(2)}) collective-permute-start(bf16[256,256]{1,0:T(8,128)(2,1)S(1)} %add_convert_fusion), channel_id=1, source_target_pairs={{0,8},{4,12},{8,0},{12,4},{16,24},{20,28},{24,16},{28,20},{1,9},{5... | collective-permute-start | bytes 393224 | tf_op jit(solution)/shard_map/ppermute | solution.py:26
  134.5 12.7 %collective-permute-start.44 = (bf16[256,256]{1,0:T(8,128)(2,1)S(1)}, bf16[256,256]{1,0:T(8,128)(2,1)S(1)}, u32[]{:S(2)}, u32[]{:S(2)}) collective-permute-start(bf16[256,256]{1,0:T(8,128)(2,1)S(1)} %get-tuple-element.103), channel_id=1, source_target_pairs={{0,16},{4,20},{8,24},{12,28},{16,0},{20,4},{24,8},{28,12},{1,17},{... | collective-permute-start | bytes 393224 | tf_op jit(solution)/shard_map/ppermute | solution.py:26
  136.8 10.4 %collective-permute-start.45 = (bf16[256,256]{1,0:T(8,128)(2,1)S(1)}, bf16[256,256]{1,0:T(8,128)(2,1)S(1)}, u32[]{:S(2)}, u32[]{:S(2)}) collective-permute-start(bf16[256,256]{1,0:T(8,128)(2,1)S(1)} %get-tuple-element.104), channel_id=1, source_target_pairs={{0,24},{4,28},{8,16},{12,20},{16,8},{20,12},{24,0},{28,4},{1,25},{... | collective-permute-start | bytes 393224 | tf_op jit(solution)/shard_map/ppermute | solution.py:26
  (28 other events, 427.9 us)
